TPU v7x, 32 devices: a whole 2x2x4 slice. The times are simulated.
32 devices in a mesh: ep: 8 (over z, x), tp: 4 (over y, core).
Axes of the slice: x: 2, y: 2, z: 4, core: 2. Of those that a mesh axis runs over, the one named last changes fastest.
Arguments:
- receptance: bfloat16 [4096, 1024], P('ep', 'tp'), may hold values from -6 to 6
- key_matrix: bfloat16 [4096, 1024], P('ep', 'tp'), may hold values from -6 to 6
- value_matrix: bfloat16 [4096, 1024], P('ep', 'tp'), may hold values from -6 to 6
- decay_data_term: bfloat16 [4096, 1024], P('ep', 'tp'), may hold values from -3.5 to 3.5
- correction_rate_data: bfloat16 [4096, 1024], P('ep', 'tp'), may hold values from -6 to 6
- output_gate_input: bfloat16 [4096, 1024], P('ep', 'tp'), may hold values from -6 to 6
- decay_channel_offset: float32 [1024], P('tp'), may hold values from -12 to -2
- correction_rate_offset: float32 [1024], P('tp'), may hold values from -12 to 1
- extra_head_log_decay: float32 [4096, 16], P('ep', 'tp'), may hold values from -2.1 to 0, as said below
- head_norm_gain: float32 [1024], P('tp'), may hold values from 0.1 to 1.9
- mixer_output_weight: bfloat16 [1024, 2048], P('tp'), may hold values from -0.1875 to 0.1875
- expert_layer_input: bfloat16 [1024, 2048], P('ep'), may hold values from -6 to 6
- feedforward_norm_gain: float32 [2048], replicated, may hold values from 0.1 to 1.9
- group_router_weight: bfloat16 [2048, 4], replicated, may hold values from -0.125 to 0.125
- expert_router_weight: bfloat16 [2048, 8], replicated, may hold values from -0.125 to 0.125
- routes: int32 [1024, 2], P('ep'), may hold values from 0 to 7, all different within a row; in each aligned block of 128 rows (0 to 127, 128 to 255, ...) at most 64 rows name the same one
- expert_gate_weight: bfloat16 [8, 2048, 4096], P('ep', None, 'tp'), may hold values from -0.125 to 0.125
- expert_up_weight: bfloat16 [8, 2048, 4096], P('ep', None, 'tp'), may hold values from -0.125 to 0.125
- expert_down_weight: bfloat16 [8, 4096, 2048], P('ep', 'tp'), may hold values from -0.09375 to 0.09375
Outputs:
- token_mixer_output: bfloat16 [4096, 2048], P(('ep', 'tp'))
- expert_out: bfloat16 [1024, 2048], P('ep', 'tp')
Inputs may be any that keep to these rules, and one draw needn't show every extreme that they name: A token's routes are distinct. Within the rows of one index of ep, no expert is named by more than 64 rows, a bound that some block reaches. `extra_head_log_decay`: entries are zero or negative; each head has a few nonzero positions.
All inputs are finite; a program needn't handle non-finite values.
Results may differ from a plain program's by a relative error of at most 0.022.
Values may be sent and summed in bfloat16 or wider, within the bound.
A program may use at most 128 MiB of HBM per device.

v0:
```python
import functools
import math

import jax
import jax.numpy as jnp
from jax import lax
from jax.experimental import pallas as pl
from jax.experimental.pallas import tpu as pltpu
from jax.sharding import PartitionSpec as P

HEAD_DIM = 64
PAIR = 2 * HEAD_DIM
BACK_LIMIT = 32 << 20
HALF_EXP = math.exp(-0.5)
GROUPS = 4


key_eps = 1e-06
group_eps = 0.00064
norm_eps = 1e-06
highest = lax.Precision.HIGHEST


def bf(x):
    return x.astype(jnp.bfloat16)


def mm(x, y):
    return lax.dot_general(x, y, (((1,), (0,)), ((), ())), preferred_element_type=jnp.float32)


def mm_nt(x, y):
    return lax.dot_general(x, y, (((1,), (1,)), ((), ())), preferred_element_type=jnp.float32)


def mm_tn(x, y):
    return lax.dot_general(x, y, (((0,), (0,)), ((), ())), preferred_element_type=jnp.float32)


def halves(x):
    high = bf(x)
    return high, bf(x - high.astype(jnp.float32))


def sum_right(x, ones):
    high, low = halves(x)
    return mm(high, ones) + mm(low, ones)


def logistic(x):
    return 1.0 / (1.0 + jnp.exp(-x))


def flag(cond):
    return jnp.where(cond, 1.0, 0.0)


def iota(shape, dim):
    return lax.broadcasted_iota(jnp.int32, shape, dim)


def pair_blocks():
    return flag((iota((PAIR, PAIR), 0) < HEAD_DIM) == (iota((PAIR, PAIR), 1) < HEAD_DIM))


def scan_kernel(
    group,
    r_ref,
    k_ref,
    v_ref,
    d_ref,
    a_ref,
    d_off_ref,
    a_off_ref,
    extra_ref,
    out_ref,
    reach_ref,
    ends_ref,
    chain_ref,
):
    positions, width = r_ref.shape
    pairs = width // PAIR
    C = HEAD_DIM
    rows_per = group * C
    own_block = pair_blocks()
    own_bf = bf(own_block)
    row, col = iota((C, PAIR), 0), iota((C, PAIR), 1) & (HEAD_DIM - 1)
    strict, upto = row > col, row >= col
    eye = flag(row == col)
    first = iota((1, PAIR), 1) < HEAD_DIM
    tri = bf(flag(iota((C, C), 0) >= iota((C, C), 1)))
    level_masks = []
    for s in range(6):
        inside = (
            ((row >> (s + 1)) == (col >> (s + 1)))
            & (((row >> s) & 1) == 1)
            & (((col >> s) & 1) == 0)
        )
        level_masks.append(bf(flag(inside)))

    def spread(x):
        return jnp.concatenate([x, x], axis=0) * own_bf

    square = (iota((PAIR, PAIR), 0) == iota((PAIR, PAIR), 1)).astype(jnp.float32)
    for p in range(pairs):
        chain_ref[p, :PAIR] = jnp.zeros((PAIR, PAIR), jnp.float32)
        chain_ref[p, PAIR:] = square

    def step(g, carry):
        base = pl.multiple_of(g * rows_per, rows_per)
        rows = pl.ds(base, rows_per)
        items = []
        for p in range(pairs):
            lanes = slice(p * PAIR, (p + 1) * PAIR)
            k = k_ref[rows, lanes].astype(jnp.float32)
            u = k * lax.rsqrt(sum_right(k * k, own_bf) + key_eps)
            rem = u * logistic(a_ref[rows, lanes].astype(jnp.float32) + a_off_ref[:, lanes])
            e = extra_ref[rows, :]
            extra = jnp.where(first, e[:, 2 * p : 2 * p + 1], e[:, 2 * p + 1 : 2 * p + 2])
            lg = extra - HALF_EXP * logistic(
                d_ref[rows, lanes].astype(jnp.float32) + d_off_ref[:, lanes]
            )
            r = r_ref[rows, lanes].astype(jnp.float32)
            v = v_ref[rows, lanes]
            for c in range(group):
                cut = slice(c * C, (c + 1) * C)
                items.append((p, c, k[cut], u[cut], rem[cut], lg[cut], r[cut], v[cut]))
        stage = []
        for p, c, k, u, rem, lg, r, v in items:
            high, low = halves(lg)
            rest = bf(lg - high.astype(jnp.float32) - low.astype(jnp.float32))
            cumul = mm(tri, high) + mm(tri, low) + mm(tri, rest)
            stage.append(cumul)
        work = []
        for (p, c, k, u, rem, lg, r, v), cumul in zip(items, stage):
            mid = 0.5 * cumul[C - 1 : C]
            up_now, down = jnp.exp(cumul - mid), jnp.exp(mid - cumul)
            up_before = jnp.exp(cumul - lg - mid)
            half = jnp.exp(mid)
            cq, cu, dk, dr = r * up_now, u * up_before, k * down, rem * down
            left = bf(jnp.concatenate([cu, cq], axis=0))
            pair_r = mm_nt(left, spread(bf(dr)))
            pair_k = mm_nt(left, spread(bf(dk)))
            work.append((cq * half, bf(cu * half), bf(dk * half), bf(dr * half), half * half, pair_r, pair_k))
        solve = []
        for (p, c, k, u, rem, lg, r, v), (qe, ue, kt, rt, ed, pair_r, pair_k) in zip(items, work):
            rp = bf(jnp.where(strict, pair_r[:C], 0.0))
            rr = bf(jnp.where(upto, pair_r[C:], 0.0))
            kp = jnp.where(strict, pair_k[:C], 0.0)
            rk = jnp.where(upto, pair_k[C:], 0.0)
            kv = mm(bf(jnp.concatenate([kp, rk], axis=0)), spread(v))
            inv = eye - (rp * level_masks[0]).astype(jnp.float32)
            solve.append([rp, rr, kv, inv])
        for s in range(1, 6):
            mids = [bf(mm(bf(inv), spread(rp * level_masks[s]))) for rp, rr, kv, inv in solve]
            for item, y in zip(solve, mids):
                item[3] = item[3] - mm(y, spread(bf(item[3])))
        wvs = []
        for (rp, rr, kv, inv), w in zip(solve, work):
            wide = jnp.concatenate([spread(w[1]), spread(bf(kv[:C]))], axis=1)
            wvs.append(bf(mm(bf(inv), wide)))
        tails = []
        for (rp, rr, kv, inv), (qe, ue, kt, rt, ed, _, _), wv, item in zip(solve, work, wvs, items):
            wide = jnp.concatenate([spread(wv[:, :PAIR]), spread(wv[:, PAIR:])], axis=1)
            rw = mm(rr, wide)
            read = bf(qe - rw[:, :PAIR])
            local = kv[C:] - rw[:, PAIR:]
            v = item[7]
            x = jnp.concatenate(
                [jnp.concatenate([v, jnp.zeros_like(v)], axis=1),
                 jnp.concatenate([-wv[:, PAIR:], -wv[:, :PAIR]], axis=1)], axis=0)
            nb = mm_tn(x, jnp.concatenate([kt, rt], axis=0))
            tails.append((read, local, nb[:PAIR] * own_block, bf(nb[PAIR:] * own_block), ed))
        z = [chain_ref[p] for p in range(pairs)]
        for c in range(group):
            for p in range(pairs):
                read, local, add, neg, ed = tails[p * group + c]
                zb = bf(z[p])
                qz = mm_nt(read, zb)
                at = pl.ds(pl.multiple_of(base + c * C, C), C)
                lanes = slice(p * PAIR, (p + 1) * PAIR)
                out_ref[at, lanes] = local + qz[:, :PAIR]
                reach_ref[at, lanes] = bf(qz[:, PAIR:])
                moved = z[p] * ed + mm(zb, neg)
                z[p] = jnp.concatenate([moved[:PAIR] + add, moved[PAIR:]], axis=0)
        for p in range(pairs):
            chain_ref[p] = z[p]
        return carry

    lax.fori_loop(0, positions // rows_per, step, 0)
    for p in range(pairs):
        s, m = chain_ref[p, :PAIR], chain_ref[p, PAIR:]
        ends_ref[p * 2 * C : p * 2 * C + C] = bf(s[:C] + s[C:])
        ends_ref[p * 2 * C + C : (p + 1) * 2 * C] = bf(m[:C] + m[C:])


def join_kernel(axis, all_ref, out_ref, reach_ref, gate_ref, gain_ref, mixed_ref):
    devices, place = lax.axis_size(axis), lax.axis_index(axis)
    width = out_ref.shape[1]
    pairs = width // PAIR
    C = HEAD_DIM
    own_block = pair_blocks()
    own_bf = bf(own_block)
    mean_bf = bf(own_block * (1.0 / HEAD_DIM))
    states = [jnp.zeros((C, PAIR), jnp.float32) for _ in range(pairs)]

    def hop(j, states):
        new = []
        for p in range(pairs):
            s = all_ref[j, p * 2 * C : p * 2 * C + C].astype(jnp.float32)
            m = all_ref[j, p * 2 * C + C : (p + 1) * 2 * C]
            m = jnp.concatenate([m, m], axis=0) * own_bf
            new.append(sum_right(states[p], m) + s)
        return tuple(new)

    states = lax.fori_loop(0, place, hop, tuple(states))
    for p in range(pairs):
        lanes = slice(p * PAIR, (p + 1) * PAIR)
        s = bf(states[p])
        s = jnp.concatenate([s, s], axis=0) * own_bf
        head = out_ref[:, lanes] + mm_nt(reach_ref[:, lanes], s)
        centred = head - sum_right(head, mean_bf)
        spread = sum_right(centred * centred, mean_bf)
        normed = centred * lax.rsqrt(spread + group_eps)
        gate = logistic(gate_ref[:, lanes].astype(jnp.float32))
        mixed_ref[:, lanes] = bf(normed * gain_ref[:, lanes] * gate)


def place_of():
    n_ep, n_tp = lax.axis_size("ep"), lax.axis_size("tp")
    e, t = lax.axis_index("ep"), lax.axis_index("tp")
    core = lax.rem(t, 2)
    return n_ep, n_tp, n_tp // 2, e, t, lax.div(t, 2), core


def remote(src, dst, send, recv, e, t):
    return pltpu.make_async_remote_copy(
        src_ref=src,
        dst_ref=dst,
        send_sem=send,
        recv_sem=recv,
        device_id=(e, t),
        device_id_type=pl.DeviceIdType.MESH,
    )


def meet():
    n_ep, n_tp, n_y, e, t, y, core = place_of()
    barrier = pltpu.get_barrier_semaphore()

    def greet(pe, pt):
        pl.semaphore_signal(
            barrier, inc=1, device_id=(pe, pt), device_id_type=pl.DeviceIdType.MESH
        )

    for d in range(1, n_ep):
        greet(lax.rem(e + d, n_ep), t)
    greet(e, 2 * y + 1 - core)
    for d in range(1, n_y):
        greet(e, 2 * lax.rem(y + d, n_y) + core)
    pl.semaphore_wait(barrier, n_ep - 1 + n_y)


def dispatch_kernel(
    group,
    r_ref,
    k_ref,
    v_ref,
    d_ref,
    a_ref,
    d_off_ref,
    a_off_ref,
    extra_ref,
    cols_ref,
    out_ref,
    reach_ref,
    piece_ref,
    every_ref,
    chain_ref,
    ends_ref,
    own_sem,
    es,
    er,
    zs,
    zr,
    gs,
    gr,
    cs,
    cr,
    ys,
    yr,
    fs,
    fr,
):
    n_ep, n_tp, n_y, e, t, y, core = place_of()
    share = cols_ref.shape[2]
    other = 2 * y + 1 - core

    def columns(index):
        return pl.ds(pl.multiple_of(index * share, share), share)

    def block(source, index):
        return piece_ref.at[source, :, columns(index)]

    meet()
    own = pltpu.make_async_copy(cols_ref.at[e], block(e, t), own_sem.at[0])
    own_ends = pltpu.make_async_copy(ends_ref, every_ref.at[e], own_sem.at[1])
    own.start()

    def ep_copy(d):
        peer = lax.rem(e + d, n_ep)
        return remote(cols_ref.at[peer], block(e, t), es.at[d], er.at[d], peer, t)

    n_x = gs.shape[0]
    n_z = n_ep // n_x
    z, x = lax.div(e, n_x), lax.rem(e, n_x)

    def up_copy(zz):
        ref = every_ref.at[zz * n_x + x]
        return remote(ref, ref, zs.at[zz], zr.at[zz], e + n_x, t)

    def side_copy(zz, h):
        ref = every_ref.at[zz * n_x + x]
        peer = z * n_x + lax.rem(x + h, n_x)
        return remote(ref, ref, gs.at[h, zz], gr.at[h, zz], peer, t)

    def pass_ends(zz):
        @pl.when(z + 1 < n_z)
        def _():
            up_copy(zz).start()

        for h in range(1, n_x):
            side_copy(zz, h).start()

    def relay_ends(i):
        @pl.when(z >= i)
        def _():
            up_copy(z - i).wait_recv()
            pass_ends(z - i)

    def close_ends(zz):
        @pl.when(z >= zz)
        def _():
            @pl.when(z + 1 < n_z)
            def _():
                up_copy(zz).wait_send()

            for h in range(1, n_x):
                side_copy(zz, h).wait()

    def source(d):
        return lax.rem(e - d + n_ep, n_ep)

    def core_copy(d):
        return remote(block(source(d), t), block(source(d), t), cs.at[d], cr.at[d], e, other)

    def y_copy(d, h):
        peer = 2 * lax.rem(y + h, n_y) + core
        return remote(block(source(d), t), block(source(d), t), ys.at[h, d], yr.at[h, d], e, peer)

    def forward_copy(d, h):
        index = 2 * lax.rem(y - h + n_y, n_y) + core
        return remote(
            block(source(d), index), block(source(d), index), fs.at[h, d], fr.at[h, d], e, other
        )

    def every(first, body, last=n_ep):
        def run(d, carry):
            body(d)
            return carry

        lax.fori_loop(first, last, run, 0)

    every(1, lambda d: ep_copy(d).start())

    def share_out(d):
        core_copy(d).start()
        for h in range(1, n_y):
            y_copy(d, h).start()

    own.wait()
    share_out(0)
    scan_kernel(
        group,
        r_ref,
        k_ref,
        v_ref,
        d_ref,
        a_ref,
        d_off_ref,
        a_off_ref,
        extra_ref,
        out_ref,
        reach_ref,
        ends_ref,
        chain_ref,
    )

    def arrived(d):
        ep_copy(d).wait_recv()
        share_out(d)

    own_ends.start()
    own_ends.wait()
    pass_ends(z)
    every(1, arrived)
    every(1, relay_ends, n_z)

    def pass_on(d):
        for h in range(1, n_y):
            y_copy(d, h).wait_recv()
            forward_copy(d, h).start()

    every(0, pass_on)

    def close(d):
        core_copy(d).wait()
        for h in range(1, n_y):
            y_copy(d, h).wait_send()
            forward_copy(d, h).wait()

    every(0, close)

    def close_far(d):
        ep_copy(d).wait_send()

    every(1, close_far)
    every(0, close_ends, n_z)


def return_kernel(
    piece_ref,
    every_ref,
    local_ref,
    reach_ref,
    gate_in_ref,
    gain_ref,
    out_weight_ref,
    gate_hbm,
    up_hbm,
    down_hbm,
    home_ref,
    mixer_ref,
    mixed_ref,
    proj_ref,
    gate_ref,
    up_ref,
    down_ref,
    rows_ref,
    hidden_ref,
    part_ref,
    near_ref,
    stage_ref,
    far_ref,
    final_ref,
    mnear_ref,
    mstage_ref,
    mfar_ref,
    gate_sem,
    up_sem,
    down_sem,
    ns,
    nr,
    ys,
    yr,
    es,
    er,
    mns,
    mnr,
    mys,
    myr,
):
    n_ep, n_tp, n_y, e, t, y, core = place_of()
    capacity, model = part_ref.shape[1:]
    units = gate_ref.shape[1]
    share = model // n_tp
    rows = proj_ref.shape[0] // (2 * n_tp)
    other = 2 * y + 1 - core
    half = n_ep // 2
    wide_units, wide_model = min(256, units), min(512, model)

    def gate_copy(i):
        at = pl.ds(pl.multiple_of(i * wide_units, wide_units), wide_units)
        return (
            pltpu.make_async_copy(gate_hbm.at[0, :, at], gate_ref.at[:, at], gate_sem.at[i]),
            pltpu.make_async_copy(up_hbm.at[0, :, at], up_ref.at[:, at], up_sem.at[i]),
        )

    def down_copy(i):
        at = pl.ds(pl.multiple_of(i * wide_model, wide_model), wide_model)
        return pltpu.make_async_copy(down_hbm.at[0, :, at], down_ref.at[:, at], down_sem.at[i])

    for i in range(units // wide_units):
        for copy in gate_copy(i):
            copy.start()
    for i in range(model // wide_model):
        down_copy(i).start()

    def columns(index):
        return pl.ds(pl.multiple_of(index * share, share), share)

    def row_block(index, q):
        return pl.ds(pl.multiple_of((2 * index + q) * rows, rows), rows)

    def peer_y(h):
        return lax.rem(y + h, n_y)

    def near_copy(s, h):
        src = part_ref.at[s, :, columns(2 * peer_y(h) + 1 - core)]
        return remote(src, near_ref.at[s, h], ns.at[s, h], nr.at[s, h], e, other)

    def y_copy(s, h):
        return remote(
            stage_ref.at[s, h], far_ref.at[s, h], ys.at[s, h], yr.at[s, h], e, 2 * peer_y(h) + core
        )

    def offset(k):
        m = lax.div(k + 1, 2)
        return lax.rem(half + m * (2 * lax.rem(k, 2) - 1) + n_ep, n_ep)

    def home_of(k):
        return lax.rem(e + offset(k), n_ep)

    def home_copy(k):
        peer, d = home_of(k), offset(k)
        return remote(final_ref.at[peer], home_ref.at[e], es.at[d], er.at[d], peer, t)

    def mnear_copy(q, h):
        src = proj_ref.at[row_block(2 * peer_y(h) + 1 - core, q), :]
        return remote(src, mnear_ref.at[q, h], mns.at[q, h], mnr.at[q, h], e, other)

    def my_copy(q, h):
        target = 2 * peer_y(h) + core
        return remote(
            mstage_ref.at[q, h], mfar_ref.at[q, h], mys.at[q, h], myr.at[q, h], e, target
        )

    def span(first, last, body):
        def run(d, carry):
            body(d)
            return carry

        lax.fori_loop(first, last, run, 0)

    def wide(x):
        return x.astype(jnp.float32)

    def mixer_sum(q, h):
        return wide(proj_ref[row_block(2 * peer_y(h) + core, q), :]) + wide(mnear_ref[q, h])

    def mixer_share(q):
        for h in range(1, n_y):
            mnear_copy(q, h).wait_recv()
            mstage_ref[q, h] = bf(mixer_sum(q, h))
            my_copy(q, h).start()

    def mixer_end(q):
        mnear_copy(q, 0).wait_recv()
        total = mixer_sum(q, 0)
        for h in range(1, n_y):
            my_copy(q, h).wait_recv()
            total = total + wide(mfar_ref[q, h])
        mixer_ref[q * rows : (q + 1) * rows] = bf(total)

    def widen(b):
        def take(k):
            at = pl.ds(pl.multiple_of((k - b * half) * capacity, capacity), capacity)
            rows_ref[at, :] = piece_ref[home_of(k)]

        span(b * half, (b + 1) * half, take)

        def unit_tile(i):
            if b == 0:
                for copy in gate_copy(i):
                    copy.wait()
            at = pl.ds(pl.multiple_of(i * wide_units, wide_units), wide_units)
            x = rows_ref[...]
            gate_val = mm(x, gate_ref[:, at])
            hidden_ref[:, at] = bf(gate_val * logistic(gate_val) * mm(x, up_ref[:, at]))

        span(0, units // wide_units, unit_tile)

    def narrow(b):
        def model_tile(i):
            if b == 0:
                down_copy(i).wait()
            at = pl.ds(pl.multiple_of(i * wide_model, wide_model), wide_model)
            result = bf(mm(hidden_ref[...], down_ref[:, at]))
            for j in range(half):
                part_ref[home_of(b * half + j), :, at] = result[j * capacity : (j + 1) * capacity]

        span(0, model // wide_model, model_tile)

    def start_near(k):
        for h in range(n_y):
            near_copy(home_of(k), h).start()

    def pair_sum(s, h):
        return wide(part_ref[s, :, columns(2 * peer_y(h) + core)]) + wide(near_ref[s, h])

    def add_near(k):
        s = home_of(k)
        for h in range(1, n_y):
            near_copy(s, h).wait_recv()
            stage_ref[s, h] = bf(pair_sum(s, h))
            y_copy(s, h).start()

    def add_far(s):
        near_copy(s, 0).wait_recv()
        total = pair_sum(s, 0)
        for h in range(1, n_y):
            y_copy(s, h).wait_recv()
            total = total + wide(far_ref[s, h])
        return bf(total)

    def go_home(k):
        s = home_of(k)
        final_ref[s] = add_far(s)
        home_copy(k).start()

    join_kernel("ep", every_ref, local_ref, reach_ref, gate_in_ref, gain_ref, mixed_ref)

    def project(i):
        at = pl.ds(pl.multiple_of(i * wide_model, wide_model), wide_model)
        proj_ref[:, at] = bf(mm(mixed_ref[...], out_weight_ref[:, at]))

    span(0, model // wide_model, project)
    meet()
    for q in range(2):
        for h in range(n_y):
            mnear_copy(q, h).start()
    mixer_share(0)
    widen(0)
    narrow(0)
    span(0, half, start_near)
    widen(1)
    span(0, half, add_near)
    narrow(1)
    span(half, n_ep, start_near)
    span(half, n_ep, add_near)
    mixer_share(1)
    span(0, half, go_home)
    mixer_end(0)
    span(half, n_ep - 1, go_home)
    home_ref[e] = add_far(e)
    mixer_end(1)

    def close(s):
        for h in range(n_y):
            near_copy(s, h).wait_send()
        for h in range(1, n_y):
            y_copy(s, h).wait_send()

    span(0, n_ep, close)
    for q in range(2):
        for h in range(n_y):
            mnear_copy(q, h).wait_send()
        for h in range(1, n_y):
            my_copy(q, h).wait_send()
    span(0, n_ep - 1, lambda k: home_copy(k).wait())


def experts_and_back(
    piece, everyone, local, reach, gate_input, gain, out_weight, gate_weight, up_weight, down_weight
):
    n_ep, n_tp = lax.axis_size("ep"), lax.axis_size("tp")
    n_y = n_tp // 2
    capacity, model = piece.shape[1:]
    units = gate_weight.shape[2]
    share, rows = model // n_tp, local.shape[0] // n_tp
    width = local.shape[1]
    out_weight = jnp.pad(out_weight, ((0, width - out_weight.shape[0]), (0, 0)))
    many, few = pltpu.SemaphoreType.DMA((n_ep, n_y)), pltpu.SemaphoreType.DMA((2, n_y))
    one = pltpu.SemaphoreType.DMA((n_ep,))

    def held(*shape):
        return pltpu.VMEM(shape, jnp.bfloat16)

    in_vmem = pl.BlockSpec(memory_space=pltpu.VMEM)
    return pl.pallas_call(
        return_kernel,
        out_shape=(
            jax.ShapeDtypeStruct((n_ep, capacity, share), jnp.bfloat16),
            jax.ShapeDtypeStruct((rows, model), jnp.bfloat16),
        ),
        in_specs=[in_vmem] * 7 + [pl.BlockSpec(memory_space=pltpu.HBM)] * 3,
        out_specs=[in_vmem] * 2,
        scratch_shapes=[
            held(*local.shape),
            held(local.shape[0], model),
            held(model, units),
            held(model, units),
            held(units, model),
            held(n_ep // 2 * capacity, model),
            held(n_ep // 2 * capacity, units),
            held(n_ep, capacity, model),
        ]
        + [held(n_ep, n_y, capacity, share)] * 3
        + [held(n_ep, capacity, share)]
        + [held(2, n_y, rows // 2, model)] * 3
        + [pltpu.SemaphoreType.DMA((max(1, units // 256),))] * 2
        + [pltpu.SemaphoreType.DMA((max(1, model // 512),))]
        + [many] * 4
        + [one] * 2
        + [few] * 4,
        compiler_params=pltpu.CompilerParams(
            collective_id=1, has_side_effects=True, vmem_limit_bytes=BACK_LIMIT
        ),
    )(
        piece,
        everyone,
        local,
        reach,
        gate_input,
        gain,
        out_weight,
        gate_weight,
        up_weight,
        down_weight,
    )


def scan_and_dispatch(
    own_columns,
    receptance,
    key_matrix,
    value_matrix,
    decay_data_term,
    correction_rate_data,
    output_gate_input,
    decay_channel_offset,
    correction_rate_offset,
    extra_head_log_decay,
    head_norm_gain,
):
    positions, own_width = receptance.shape
    pairs = -(-own_width // PAIR)
    width = pairs * PAIR

    def filled(x, columns=width):
        return x if x.shape[-1] == columns else jnp.pad(x, ((0, 0), (0, columns - x.shape[-1])))

    blocks = positions // HEAD_DIM
    group = 4 if blocks % 4 == 0 else 1
    n_ep, n_tp = lax.axis_size("ep"), lax.axis_size("tp")
    n_y = n_tp // 2
    n_x = 1
    while 4 * n_x * n_x <= n_ep:
        n_x = 2 * n_x
    capacity, share = own_columns.shape[1:]
    ends = (pairs * 2 * HEAD_DIM, PAIR)
    one, many = pltpu.SemaphoreType.DMA((n_ep,)), pltpu.SemaphoreType.DMA((n_y, n_ep))
    local, reach, piece, everyone = pl.pallas_call(
        functools.partial(dispatch_kernel, group),
        out_shape=(
            jax.ShapeDtypeStruct((positions, width), jnp.float32),
            jax.ShapeDtypeStruct((positions, width), jnp.bfloat16),
            jax.ShapeDtypeStruct((n_ep, capacity, n_tp * share), jnp.bfloat16),
            jax.ShapeDtypeStruct((n_ep, *ends), jnp.bfloat16),
        ),
        in_specs=[pl.BlockSpec(memory_space=pltpu.VMEM)] * 9,
        out_specs=[pl.BlockSpec(memory_space=pltpu.VMEM)] * 4,
        scratch_shapes=[
            pltpu.VMEM((pairs, 2 * PAIR, PAIR), jnp.float32),
            pltpu.VMEM(ends, jnp.bfloat16),
            pltpu.SemaphoreType.DMA((2,)),
        ]
        + [one] * 2
        + [pltpu.SemaphoreType.DMA((n_ep // n_x,))] * 2
        + [pltpu.SemaphoreType.DMA((n_x, n_ep // n_x))] * 2
        + [one] * 2
        + [many] * 4,
        compiler_params=pltpu.CompilerParams(
            collective_id=0, has_side_effects=True, vmem_limit_bytes=16 << 20
        ),
        cost_estimate=pl.CostEstimate(
            flops=200000 * positions * width,
            bytes_accessed=16 * positions * width,
            transcendentals=0,
        ),
    )(
        filled(receptance),
        filled(key_matrix),
        filled(value_matrix),
        filled(decay_data_term),
        filled(correction_rate_data),
        filled(decay_channel_offset[None]),
        filled(correction_rate_offset[None]),
        filled(extra_head_log_decay, 2 * pairs),
        own_columns,
    )
    gate_input, gain = filled(output_gate_input), filled(head_norm_gain[None])
    return local, reach, piece, everyone, gate_input, gain


def expert_route(
    expert_layer_input,
    feedforward_norm_gain,
    group_router_weight,
    expert_router_weight,
    routes,
):
    token_rows = expert_layer_input.shape[0]
    route_count = routes.shape[1]
    ep_count = lax.axis_size("ep")
    expert_total = expert_router_weight.shape[1]
    per_group = expert_total // GROUPS
    capacity = 4 * token_rows // ep_count
    widened = expert_layer_input.astype(jnp.float32)
    normed_input = (
        widened
        * lax.rsqrt(jnp.mean(widened * widened, axis=-1, keepdims=True) + norm_eps)
        * feedforward_norm_gain
    ).astype(jnp.bfloat16)
    group_logit = jnp.dot(normed_input, group_router_weight, preferred_element_type=jnp.float32)
    group_exp = jnp.exp(group_logit)
    group_prob = group_exp / jnp.sum(group_exp, axis=-1, keepdims=True)
    expert_logit = jnp.dot(normed_input, expert_router_weight, preferred_element_type=jnp.float32)
    expert_range = jnp.arange(expert_total, dtype=jnp.int32)
    matched = routes[:, :, None] == expert_range[None, None, :]
    chosen_logit = jnp.sum(jnp.where(matched, expert_logit[:, None, :], 0.0), axis=-1)
    group_match = (routes // per_group)[:, :, None] == jnp.arange(GROUPS, dtype=jnp.int32)[
        None, None, :
    ]
    chosen_group = jnp.sum(jnp.where(group_match, group_prob[:, None, :], 0.0), axis=-1)
    route_weight = chosen_group * jax.nn.sigmoid(chosen_logit - chosen_logit[:, ::-1])
    flat_match = matched.reshape(token_rows * route_count, expert_total).astype(jnp.int32)
    before = jnp.cumsum(flat_match, axis=0) - flat_match
    placed = jnp.sum(before * flat_match, axis=1)
    slot_ids = routes.reshape(-1) * capacity + placed
    slot_range = jnp.arange(expert_total * capacity, dtype=jnp.int32)
    struck = (slot_range[:, None] == slot_ids[None, :]).reshape(
        expert_total * capacity, token_rows, route_count
    )
    dispatch_matrix = jnp.any(struck, axis=-1).astype(jnp.bfloat16)
    combine_matrix = jnp.sum(jnp.where(struck, route_weight[None, :, :], 0.0), axis=-1)
    outgoing = jnp.dot(dispatch_matrix, normed_input, preferred_element_type=jnp.float32).astype(
        jnp.bfloat16
    )
    outgoing = outgoing.reshape(ep_count, capacity, outgoing.shape[1])
    width_share = outgoing.shape[2] // lax.axis_size("tp")
    own_columns = lax.dynamic_slice_in_dim(
        outgoing, lax.axis_index("tp") * width_share, width_share, 2
    )
    return own_columns, combine_matrix


def expert_combine(homebound, combine_matrix):
    homebound = homebound.reshape(-1, homebound.shape[2]).astype(jnp.float32)
    combined = lax.dot_general(
        combine_matrix, homebound, (((0,), (0,)), ((), ())), precision=highest
    )
    return combined.astype(jnp.bfloat16)


def local(
    receptance,
    key_matrix,
    value_matrix,
    decay_data_term,
    correction_rate_data,
    output_gate_input,
    decay_channel_offset,
    correction_rate_offset,
    extra_head_log_decay,
    head_norm_gain,
    mixer_output_weight,
    expert_layer_input,
    feedforward_norm_gain,
    group_router_weight,
    expert_router_weight,
    routes,
    expert_gate_weight,
    expert_up_weight,
    expert_down_weight,
):
    own_columns, combine_matrix = expert_route(
        expert_layer_input,
        feedforward_norm_gain,
        group_router_weight,
        expert_router_weight,
        routes,
    )
    local_read, reach, piece, everyone, gate_input, gain = scan_and_dispatch(
        own_columns,
        receptance,
        key_matrix,
        value_matrix,
        decay_data_term,
        correction_rate_data,
        output_gate_input,
        decay_channel_offset,
        correction_rate_offset,
        extra_head_log_decay,
        head_norm_gain,
    )
    homebound, token_mixer_output = experts_and_back(
        piece,
        everyone,
        local_read,
        reach,
        gate_input,
        gain,
        mixer_output_weight,
        expert_gate_weight,
        expert_up_weight,
        expert_down_weight,
    )
    return (token_mixer_output, expert_combine(homebound, combine_matrix))


def solution(mesh):
    in_specs = (
        P("ep", "tp"),
        P("ep", "tp"),
        P("ep", "tp"),
        P("ep", "tp"),
        P("ep", "tp"),
        P("ep", "tp"),
        P("tp"),
        P("tp"),
        P("ep", "tp"),
        P("tp"),
        P("tp", None),
        P("ep", None),
        P(),
        P(),
        P(),
        P("ep", None),
        P("ep", None, "tp"),
        P("ep", None, "tp"),
        P("ep", "tp", None),
    )
    out_specs = (P(("ep", "tp"), None), P("ep", "tp"))
    return jax.shard_map(local, mesh=mesh, in_specs=in_specs, out_specs=out_specs, check_vma=False)
```

profile of v0, /device:TPU:0, one launch (start us, length us, event | category | flops | bytes accessed | tf_op | source)
XLA Modules:
  0.0 77.8 jit_solution(5647268120862471368)
XLA Ops:
  0.6 0.0 copy-start
  0.7 0.9 %copy.42 = s32[128,2]{1,0:T(8,128)S(1)} copy(s32[128,2]{0,1:T(2,128)} %param.34) | data formatting | bytes 2048 | tf_op args[15]
  1.6 0.1 eq.64
  1.8 0.6 reduce-window.6
  2.4 0.2 slice_reduce_fusion
  2.6 0.1 eq.60
  2.8 0.1 fusion.5
  2.8 0.1 reduce_sum.57
  3.0 0.1 copy.44
  3.1 0.7 and_select_fusion
  3.8 0.1 fusion.3
  3.8 1.2 %fusion = f32[128]{0:T(128)S(1)} fusion(bf16[128,2048]{1,0:T(8,128)(2,1)} %param.30), kind=kLoop, calls=%fused_computation.5 | loop fusion | flops 786304 | bytes 524800 | tf_op jit(solution)/shard_map/reduce_sum | solution.py:812
  5.1 3.2 %convolution_convert_fusion = bf16[512,2048]{1,0:T(8,128)(2,1)} fusion(pred[512,128]{1,0:T(8,128)(4,1)S(1)} %fusion.3, bf16[128,2048]{1,0:T(8,128)(2,1)} %param.30, f32[2048]{0:T(1024)} %param.31, f32[128]{0:T(128)S(1)} %add_rsqrt_fusion), kind=kOutput, calls=%fused_computation | convolution fusion | flops 270532608 | bytes 2695680 | tf_op jit(solution)/shard_map/dot_general | solution.py:837
  8.2 1.1 %constant_dynamic-slice_fusion.cols_ref = bf16[8,64,512]{2,1,0:T(8,128)(2,1)S(1)} fusion(bf16[8,64,2048]{2,1,0:T(8,128)(2,1)} %bitcast.22, s32[]{:T(128)S(6)} %select_n.20), kind=kLoop, calls=%fused_computation.30 | loop fusion | bytes 1048580 | tf_op jit(solution)/shard_map/dynamic_slice | solution.py:842
  9.4 0.1 copy.45.extra_ref
  9.6 0.0 copy-start.1
  9.6 0.0 copy-start.2
  9.6 0.0 copy-start.3
  9.6 0.0 copy-start.4
  9.6 0.0 copy-start.5
  9.6 0.0 copy-start.6
  9.6 26.2 %shard_map.194 = (f32[512,256]{1,0:T(8,128)S(1)}, bf16[512,256]{1,0:T(8,128)(2,1)S(1)}, bf16[8,64,2048]{2,1,0:T(8,128)(2,1)S(1)}, bf16[8,256,128]{2,1,0:T(8,128)(2,1)S(1)}) custom-call(bf16[512,256]{1,0:T(8,128)(2,1)S(1)} %copy-done.7, bf16[512,256]{1,0:T(8,128)(2,1)S(1)} %copy-done.8, bf16[512,256]{1,0:T(8,128)(2,1)S(1)} %copy-done.9, ...), custom_call_target="tpu_custom_call" | custom-call | flops 26214400000 | bytes 2097152 | tf_op jit(solution)/shard_map/pallas_call | solution.py:753
  35.9 0.0 copy-start.14
  35.9 0.0 copy-start.16
  36.0 0.0 copy-start.18
  36.0 0.0 copy-start.15
  36.0 39.1 %shard_map.195 = (bf16[8,64,512]{2,1,0:T(8,128)(2,1)S(1)}, bf16[128,2048]{1,0:T(8,128)(2,1)S(1)}) custom-call(bf16[8,64,2048]{2,1,0:T(8,128)(2,1)S(1)} %get-tuple-element.8.piece_ref, bf16[8,256,128]{2,1,0:T(8,128)(2,1)S(1)} %get-tuple-element.9.every_ref, f32[512,256]{1,0:T(8,128)S(1)} %get-tuple-element.10.local_ref, ...), custom_call_target="tpu_custom_call" | custom-call | tf_op jit(solution)/shard_map/pallas_call | solution.py:680
  75.1 0.3 fusion.11
  75.5 0.3 fusion.7
  75.8 0.1 select_reduce_fusion
  75.9 1.1 %convolution_convert_fusion.1 = bf16[128,512]{1,0:T(8,128)(2,1)} fusion(f32[512,128]{1,0:T(8,128)S(1)} %select_reduce_fusion, bf16[512,512]{1,0:T(8,128)(2,1)S(1)} %bitcast.18), kind=kOutput, calls=%fused_computation.3 | convolution fusion | flops 402718720 | bytes 917504 | tf_op jit(solution)/shard_map/dot_general | solution.py:850
  77.0 0.8 %copy.47 = bf16[128,2048]{1,0:T(8,128)(2,1)} copy(bf16[128,2048]{1,0:T(8,128)(2,1)S(1)} %get-tuple-element.20) | data formatting | bytes 1048576
  (36 shorter events, 0.2 us)
Async XLA Ops:
  0.6 74.8 %copy-start = (bf16[2048,8]{0,1:T(8,128)(2,1)S(1)}, bf16[2048,8]{0,1:T(8,128)(2,1)}, u32[]{:S(2)}) copy-start(bf16[2048,8]{0,1:T(8,128)(2,1)} %param.33) | copy-start | bytes 98308
  0.6 8.7 %copy-start.17 = (f32[512,4]{0,1:T(4,128)S(1)}, f32[512,4]{0,1:T(4,128)}, u32[]{:S(2)}) copy-start(f32[512,4]{0,1:T(4,128)} %param.27) | copy-start | bytes 24580
  0.7 8.8 %copy-start.12 = (f32[256]{0:T(256)S(1)}, f32[256]{0:T(256)}, u32[]{:S(2)}) copy-start(f32[256]{0:T(256)} %param.25) | copy-start | bytes 3076
  0.7 8.8 %copy-start.13 = (f32[256]{0:T(256)S(1)}, f32[256]{0:T(256)}, u32[]{:S(2)}) copy-start(f32[256]{0:T(256)} %param.26) | copy-start | bytes 3076
  0.7 8.8 %copy-start.7 = (bf16[512,256]{1,0:T(8,128)(2,1)S(1)}, bf16[512,256]{1,0:T(8,128)(2,1)}, u32[]{:S(2)}) copy-start(bf16[512,256]{1,0:T(8,128)(2,1)} %r_ref.1) | copy-start | bytes 786436
  0.7 8.8 %copy-start.8 = (bf16[512,256]{1,0:T(8,128)(2,1)S(1)}, bf16[512,256]{1,0:T(8,128)(2,1)}, u32[]{:S(2)}) copy-start(bf16[512,256]{1,0:T(8,128)(2,1)} %k_ref.1) | copy-start | bytes 786436
  0.7 8.8 %copy-start.9 = (bf16[512,256]{1,0:T(8,128)(2,1)S(1)}, bf16[512,256]{1,0:T(8,128)(2,1)}, u32[]{:S(2)}) copy-start(bf16[512,256]{1,0:T(8,128)(2,1)} %v_ref.1) | copy-start | bytes 786436
  0.7 8.8 %copy-start.10 = (bf16[512,256]{1,0:T(8,128)(2,1)S(1)}, bf16[512,256]{1,0:T(8,128)(2,1)}, u32[]{:S(2)}) copy-start(bf16[512,256]{1,0:T(8,128)(2,1)} %d_ref.1) | copy-start | bytes 786436
  0.7 8.8 %copy-start.11 = (bf16[512,256]{1,0:T(8,128)(2,1)S(1)}, bf16[512,256]{1,0:T(8,128)(2,1)}, u32[]{:S(2)}) copy-start(bf16[512,256]{1,0:T(8,128)(2,1)} %a_ref.1) | copy-start | bytes 786436
  9.6 26.3 %copy-start.1 = (bf16[1,2048,1024]{2,1,0:T(8,128)(2,1)S(1)}, bf16[1,2048,1024]{2,1,0:T(8,128)(2,1)}, u32[]{:S(2)}) copy-start(bf16[1,2048,1024]{2,1,0:T(8,128)(2,1)} %gate_hbm.1) | copy-start | bytes 12582916
  9.6 26.3 %copy-start.2 = (bf16[1,2048,1024]{2,1,0:T(8,128)(2,1)S(1)}, bf16[1,2048,1024]{2,1,0:T(8,128)(2,1)}, u32[]{:S(2)}) copy-start(bf16[1,2048,1024]{2,1,0:T(8,128)(2,1)} %up_hbm.1) | copy-start | bytes 12582916
  9.6 26.3 %copy-start.3 = (bf16[1,1024,2048]{2,1,0:T(8,128)(2,1)S(1)}, bf16[1,1024,2048]{2,1,0:T(8,128)(2,1)}, u32[]{:S(2)}) copy-start(bf16[1,1024,2048]{2,1,0:T(8,128)(2,1)} %down_hbm.1) | copy-start | bytes 12582916
  9.6 26.3 %copy-start.4 = (bf16[256,2048]{1,0:T(8,128)(2,1)S(1)}, bf16[256,2048]{1,0:T(8,128)(2,1)}, u32[]{:S(2)}) copy-start(bf16[256,2048]{1,0:T(8,128)(2,1)} %out_weight_ref.1) | copy-start | bytes 3145732
  9.6 26.3 %copy-start.5 = (bf16[512,256]{1,0:T(8,128)(2,1)S(1)}, bf16[512,256]{1,0:T(8,128)(2,1)}, u32[]{:S(2)}) copy-start(bf16[512,256]{1,0:T(8,128)(2,1)} %gate_in_ref.1) | copy-start | bytes 786436
  9.6 26.3 %copy-start.6 = (f32[256]{0:T(256)S(1)}, f32[256]{0:T(256)}, u32[]{:S(2)}) copy-start(f32[256]{0:T(256)} %param.28) | copy-start | bytes 3076
  35.9 39.1 %copy-start.14 = (bf16[128,2048]{1,0:T(8,128)(2,1)S(1)}, bf16[128,2048]{1,0:T(8,128)(2,1)}, u32[]{:S(2)}) copy-start(bf16[128,2048]{1,0:T(8,128)(2,1)} %param.30) | copy-start | bytes 1572868
  35.9 39.1 %copy-start.16 = (f32[2048]{0:T(1024)S(1)}, f32[2048]{0:T(1024)}, u32[]{:S(2)}) copy-start(f32[2048]{0:T(1024)} %param.31) | copy-start | bytes 24580
  36.0 39.1 %copy-start.18 = (bf16[2048,4]{0,1:T(4,128)(2,1)S(1)}, bf16[2048,4]{0,1:T(4,128)(2,1)}, u32[]{:S(2)}) copy-start(bf16[2048,4]{0,1:T(4,128)(2,1)} %param.32) | copy-start | bytes 49156
  36.0 39.8 %copy-start.15 = (s32[128,2]{0,1:T(2,128)S(1)}, s32[128,2]{0,1:T(2,128)}, u32[]{:S(2)}) copy-start(s32[128,2]{0,1:T(2,128)} %param.34) | copy-start | bytes 3076
where the time goes:
time: 78.3 us; the launch traced here: 77.8 us
  Pallas kernels  65.3 us (83%)
  matrix products  4.91 us (6%)
  local copies, waits for them, and re-layouts  3.74 us (5%)
  other arithmetic  2.87 us (4%)
  between operations  1.01 us (1%)
    pallas_call x1, Pallas kernels, experts_and_back(): pl.pallas_call(return_kernel, out_shape=(jax.ShapeDtypeStruct((n_ep, capa...  39.1 us
    pallas_call x1, Pallas kernels, scan_and_dispatch(): pl.pallas_call(functools.partial(dispatch_kernel, group), out_shape=(jax....  26.2 us
    dot_general x1, matrix products, expert_route(): jnp.dot(dispatch_matrix, normed_input, preferred_element_type=jnp.float32)  3.18 us
    unnamed x41, local copies, waits for them, and re-layouts  1.93 us

commit v1 on v0

v1 whole, which is shorter than its diff:
```python
import functools
import math

import jax
import jax.numpy as jnp
from jax import lax
from jax.experimental import pallas as pl
from jax.experimental.pallas import tpu as pltpu
from jax.sharding import PartitionSpec as P

HEAD_DIM = 64
PAIR = 2 * HEAD_DIM
VMEM_LIMIT = 56 << 20
HALF_EXP = math.exp(-0.5)
GROUPS = 4


key_eps = 1e-06
group_eps = 0.00064
norm_eps = 1e-06
highest = lax.Precision.HIGHEST


def bf(x):
    return x.astype(jnp.bfloat16)


def mm(x, y):
    return lax.dot_general(x, y, (((1,), (0,)), ((), ())), preferred_element_type=jnp.float32)


def mm_nt(x, y):
    return lax.dot_general(x, y, (((1,), (1,)), ((), ())), preferred_element_type=jnp.float32)


def mm_tn(x, y):
    return lax.dot_general(x, y, (((0,), (0,)), ((), ())), preferred_element_type=jnp.float32)


def halves(x):
    high = bf(x)
    return high, bf(x - high.astype(jnp.float32))


def sum_right(x, ones):
    high, low = halves(x)
    return mm(high, ones) + mm(low, ones)


def logistic(x):
    return 1.0 / (1.0 + jnp.exp(-x))


def flag(cond):
    return jnp.where(cond, 1.0, 0.0)


def iota(shape, dim):
    return lax.broadcasted_iota(jnp.int32, shape, dim)


def pair_blocks():
    return flag((iota((PAIR, PAIR), 0) < HEAD_DIM) == (iota((PAIR, PAIR), 1) < HEAD_DIM))


def scan_kernel(
    group,
    pump,
    r_ref,
    k_ref,
    v_ref,
    d_ref,
    a_ref,
    d_off_ref,
    a_off_ref,
    extra_ref,
    out_ref,
    reach_ref,
    ends_ref,
    chain_ref,
):
    positions, width = r_ref.shape
    pairs = width // PAIR
    C = HEAD_DIM
    rows_per = group * C
    own_block = pair_blocks()
    own_bf = bf(own_block)
    row, col = iota((C, PAIR), 0), iota((C, PAIR), 1) & (HEAD_DIM - 1)
    strict, upto = row > col, row >= col
    eye = flag(row == col)
    first = iota((1, PAIR), 1) < HEAD_DIM
    tri = bf(flag(iota((C, C), 0) >= iota((C, C), 1)))
    level_masks = []
    for s in range(6):
        inside = (
            ((row >> (s + 1)) == (col >> (s + 1)))
            & (((row >> s) & 1) == 1)
            & (((col >> s) & 1) == 0)
        )
        level_masks.append(bf(flag(inside)))

    def spread(x):
        return jnp.concatenate([x, x], axis=0) * own_bf

    square = (iota((PAIR, PAIR), 0) == iota((PAIR, PAIR), 1)).astype(jnp.float32)
    for p in range(pairs):
        chain_ref[p, :PAIR] = jnp.zeros((PAIR, PAIR), jnp.float32)
        chain_ref[p, PAIR:] = square

    def step(g, carry):
        base = pl.multiple_of(g * rows_per, rows_per)
        rows = pl.ds(base, rows_per)
        items = []
        for p in range(pairs):
            lanes = slice(p * PAIR, (p + 1) * PAIR)
            k = k_ref[rows, lanes].astype(jnp.float32)
            u = k * lax.rsqrt(sum_right(k * k, own_bf) + key_eps)
            rem = u * logistic(a_ref[rows, lanes].astype(jnp.float32) + a_off_ref[:, lanes])
            e = extra_ref[rows, :]
            extra = jnp.where(first, e[:, 2 * p : 2 * p + 1], e[:, 2 * p + 1 : 2 * p + 2])
            lg = extra - HALF_EXP * logistic(
                d_ref[rows, lanes].astype(jnp.float32) + d_off_ref[:, lanes]
            )
            r = r_ref[rows, lanes].astype(jnp.float32)
            v = v_ref[rows, lanes]
            for c in range(group):
                cut = slice(c * C, (c + 1) * C)
                items.append((p, c, k[cut], u[cut], rem[cut], lg[cut], r[cut], v[cut]))
        stage = []
        for p, c, k, u, rem, lg, r, v in items:
            high, low = halves(lg)
            rest = bf(lg - high.astype(jnp.float32) - low.astype(jnp.float32))
            cumul = mm(tri, high) + mm(tri, low) + mm(tri, rest)
            stage.append(cumul)
        work = []
        for (p, c, k, u, rem, lg, r, v), cumul in zip(items, stage):
            mid = 0.5 * cumul[C - 1 : C]
            up_now, down = jnp.exp(cumul - mid), jnp.exp(mid - cumul)
            up_before = jnp.exp(cumul - lg - mid)
            half = jnp.exp(mid)
            cq, cu, dk, dr = r * up_now, u * up_before, k * down, rem * down
            left = bf(jnp.concatenate([cu, cq], axis=0))
            pair_r = mm_nt(left, spread(bf(dr)))
            pair_k = mm_nt(left, spread(bf(dk)))
            work.append((cq * half, bf(cu * half), bf(dk * half), bf(dr * half), half * half, pair_r, pair_k))
        pump(g, 0)
        solve = []
        for (p, c, k, u, rem, lg, r, v), (qe, ue, kt, rt, ed, pair_r, pair_k) in zip(items, work):
            rp = bf(jnp.where(strict, pair_r[:C], 0.0))
            rr = bf(jnp.where(upto, pair_r[C:], 0.0))
            kp = jnp.where(strict, pair_k[:C], 0.0)
            rk = jnp.where(upto, pair_k[C:], 0.0)
            kv = mm(bf(jnp.concatenate([kp, rk], axis=0)), spread(v))
            inv = eye - (rp * level_masks[0]).astype(jnp.float32)
            solve.append([rp, rr, kv, inv])
        for s in range(1, 6):
            mids = [bf(mm(bf(inv), spread(rp * level_masks[s]))) for rp, rr, kv, inv in solve]
            for item, y in zip(solve, mids):
                item[3] = item[3] - mm(y, spread(bf(item[3])))
            if s == 2:
                pump(g, 1)
        wvs = []
        for (rp, rr, kv, inv), w in zip(solve, work):
            wide = jnp.concatenate([spread(w[1]), spread(bf(kv[:C]))], axis=1)
            wvs.append(bf(mm(bf(inv), wide)))
        pump(g, 2)
        tails = []
        for (rp, rr, kv, inv), (qe, ue, kt, rt, ed, _, _), wv, item in zip(solve, work, wvs, items):
            wide = jnp.concatenate([spread(wv[:, :PAIR]), spread(wv[:, PAIR:])], axis=1)
            rw = mm(rr, wide)
            read = bf(qe - rw[:, :PAIR])
            local = kv[C:] - rw[:, PAIR:]
            v = item[7]
            x = jnp.concatenate(
                [jnp.concatenate([v, jnp.zeros_like(v)], axis=1),
                 jnp.concatenate([-wv[:, PAIR:], -wv[:, :PAIR]], axis=1)], axis=0)
            nb = mm_tn(x, jnp.concatenate([kt, rt], axis=0))
            tails.append((read, local, nb[:PAIR] * own_block, bf(nb[PAIR:] * own_block), ed))
        z = [chain_ref[p] for p in range(pairs)]
        for c in range(group):
            for p in range(pairs):
                read, local, add, neg, ed = tails[p * group + c]
                zb = bf(z[p])
                qz = mm_nt(read, zb)
                at = pl.ds(pl.multiple_of(base + c * C, C), C)
                lanes = slice(p * PAIR, (p + 1) * PAIR)
                out_ref[at, lanes] = local + qz[:, :PAIR]
                reach_ref[at, lanes] = bf(qz[:, PAIR:])
                moved = z[p] * ed + mm(zb, neg)
                z[p] = jnp.concatenate([moved[:PAIR] + add, moved[PAIR:]], axis=0)
        for p in range(pairs):
            chain_ref[p] = z[p]
        pump(g, 3)
        return carry

    lax.fori_loop(0, positions // rows_per, step, 0)
    for p in range(pairs):
        s, m = chain_ref[p, :PAIR], chain_ref[p, PAIR:]
        ends_ref[p * 2 * C : p * 2 * C + C] = bf(s[:C] + s[C:])
        ends_ref[p * 2 * C + C : (p + 1) * 2 * C] = bf(m[:C] + m[C:])


def join_kernel(axis, all_ref, out_ref, reach_ref, gate_ref, gain_ref, mixed_ref):
    devices, place = lax.axis_size(axis), lax.axis_index(axis)
    width = out_ref.shape[1]
    pairs = width // PAIR
    C = HEAD_DIM
    own_block = pair_blocks()
    own_bf = bf(own_block)
    mean_bf = bf(own_block * (1.0 / HEAD_DIM))
    states = [jnp.zeros((C, PAIR), jnp.float32) for _ in range(pairs)]

    def hop(j, states):
        new = []
        for p in range(pairs):
            s = all_ref[j, p * 2 * C : p * 2 * C + C].astype(jnp.float32)
            m = all_ref[j, p * 2 * C + C : (p + 1) * 2 * C]
            m = jnp.concatenate([m, m], axis=0) * own_bf
            new.append(sum_right(states[p], m) + s)
        return tuple(new)

    states = lax.fori_loop(0, place, hop, tuple(states))
    for p in range(pairs):
        lanes = slice(p * PAIR, (p + 1) * PAIR)
        s = bf(states[p])
        s = jnp.concatenate([s, s], axis=0) * own_bf
        head = out_ref[:, lanes] + mm_nt(reach_ref[:, lanes], s)
        centred = head - sum_right(head, mean_bf)
        spread = sum_right(centred * centred, mean_bf)
        normed = centred * lax.rsqrt(spread + group_eps)
        gate = logistic(gate_ref[:, lanes].astype(jnp.float32))
        mixed_ref[:, lanes] = bf(normed * gain_ref[:, lanes] * gate)


def place_of():
    n_ep, n_tp = lax.axis_size("ep"), lax.axis_size("tp")
    e, t = lax.axis_index("ep"), lax.axis_index("tp")
    core = lax.rem(t, 2)
    return n_ep, n_tp, n_tp // 2, e, t, lax.div(t, 2), core


def remote(src, dst, send, recv, e, t):
    return pltpu.make_async_remote_copy(
        src_ref=src,
        dst_ref=dst,
        send_sem=send,
        recv_sem=recv,
        device_id=(e, t),
        device_id_type=pl.DeviceIdType.MESH,
    )


def meet():
    n_ep, n_tp, n_y, e, t, y, core = place_of()
    barrier = pltpu.get_barrier_semaphore()

    def greet(pe, pt):
        pl.semaphore_signal(
            barrier, inc=1, device_id=(pe, pt), device_id_type=pl.DeviceIdType.MESH
        )

    for d in range(1, n_ep):
        greet(lax.rem(e + d, n_ep), t)
    greet(e, 2 * y + 1 - core)
    for d in range(1, n_y):
        greet(e, 2 * lax.rem(y + d, n_y) + core)
    return lambda: pl.semaphore_wait(barrier, n_ep - 1 + n_y)


def span(first, last, body):
    def run(d, carry):
        body(d)
        return carry

    lax.fori_loop(first, last, run, 0)


def wide(x):
    return x.astype(jnp.float32)


def whole_kernel(
    group,
    r_hbm,
    k_hbm,
    v_hbm,
    d_hbm,
    a_hbm,
    gate_in_hbm,
    d_off_ref,
    a_off_ref,
    extra_ref,
    gain_ref,
    out_weight_hbm,
    x_hbm,
    norm_gain_ref,
    group_router_ref,
    expert_router_ref,
    routes_ref,
    gate_hbm,
    up_hbm,
    down_hbm,
    mixer_ref,
    expert_ref,
    r_ref,
    k_ref,
    v_ref,
    d_ref,
    a_ref,
    gate_in_ref,
    out_weight_ref,
    x_ref,
    normed_ref,
    place_ref,
    cols_ref,
    piece_ref,
    out_ref,
    reach_ref,
    every_ref,
    chain_ref,
    mixed_ref,
    proj_ref,
    gate_ref,
    up_ref,
    down_ref,
    hidden_ref,
    part_ref,
    near_ref,
    stage_ref,
    far_ref,
    final_ref,
    home_ref,
    mnear_ref,
    mstage_ref,
    mfar_ref,
    in_sem,
    gate_sem,
    up_sem,
    down_sem,
    es,
    er,
    cs,
    cr,
    ys,
    yr,
    fs,
    fr,
    zs,
    zr,
    gs,
    gr,
    ns,
    nr,
    bs,
    br,
    hs,
    hr,
    mns,
    mnr,
    mys,
    myr,
):
    n_ep, n_tp, n_y, e, t, y, core = place_of()
    units = gate_ref.shape[1]
    model = x_ref.shape[1]
    tokens = x_ref.shape[0]
    share = model // n_tp
    slots = piece_ref.shape[0]
    capacity = slots // n_ep
    experts = expert_router_ref.shape[0]
    groups = group_router_ref.shape[0]
    rows = proj_ref.shape[0] // (2 * n_tp)
    other = 2 * y + 1 - core
    half = n_ep // 2
    half_rows = half * capacity
    wide_units, wide_model = min(256, units), min(512, model)

    inputs = [(x_hbm, x_ref)]
    inputs += [(k_hbm, k_ref), (a_hbm, a_ref), (d_hbm, d_ref), (r_hbm, r_ref), (v_hbm, v_ref)]
    inputs += [(gate_in_hbm, gate_in_ref), (out_weight_hbm, out_weight_ref)]
    loads = [pltpu.make_async_copy(s, d, in_sem.at[i]) for i, (s, d) in enumerate(inputs)]

    def gate_copy(i):
        at = pl.ds(pl.multiple_of(i * wide_units, wide_units), wide_units)
        return (
            pltpu.make_async_copy(gate_hbm.at[0, :, at], gate_ref.at[:, at], gate_sem.at[i]),
            pltpu.make_async_copy(up_hbm.at[0, :, at], up_ref.at[:, at], up_sem.at[i]),
        )

    def down_copy(i):
        at = pl.ds(pl.multiple_of(i * wide_model, wide_model), wide_model)
        return pltpu.make_async_copy(down_hbm.at[0, :, at], down_ref.at[:, at], down_sem.at[i])

    def columns(index):
        return pl.ds(pl.multiple_of(index * share, share), share)

    def block(d):
        return pl.ds(pl.multiple_of(d * capacity, capacity), capacity)

    def peer_y(h):
        return lax.rem(y + h, n_y)

    def ep_copy(d):
        peer = lax.rem(e + d, n_ep)
        return remote(
            cols_ref.at[block(peer), :], piece_ref.at[block(d), columns(t)], es.at[d], er.at[d], peer, t
        )

    def core_copy(d):
        ref = piece_ref.at[block(d), columns(t)]
        return remote(ref, ref, cs.at[d], cr.at[d], e, other)

    def y_copy(d, h):
        ref = piece_ref.at[block(d), columns(t)]
        return remote(ref, ref, ys.at[h, d], yr.at[h, d], e, 2 * peer_y(h) + core)

    def forward_copy(d, h):
        ref = piece_ref.at[block(d), columns(2 * lax.rem(y - h + n_y, n_y) + core)]
        return remote(ref, ref, fs.at[h, d], fr.at[h, d], e, other)

    def arrived(d):
        ep_copy(d).wait_recv()
        for h in range(1, n_y):
            y_copy(d, h).start()
        core_copy(d).start()

    def pass_on(d):
        for h in range(1, n_y):
            y_copy(d, h).wait_recv()
            forward_copy(d, h).start()

    def gathered(d):
        core_copy(d).wait_recv()
        for h in range(1, n_y):
            forward_copy(d, h).wait_recv()

    n_x = gs.shape[0]
    n_z = n_ep // n_x
    z, x = lax.div(e, n_x), lax.rem(e, n_x)

    def up_copy(zz):
        ref = every_ref.at[zz * n_x + x]
        return remote(ref, ref, zs.at[zz], zr.at[zz], e + n_x, t)

    def side_copy(zz, h):
        ref = every_ref.at[zz * n_x + x]
        peer = z * n_x + lax.rem(x + h, n_x)
        return remote(ref, ref, gs.at[h, zz], gr.at[h, zz], peer, t)

    def pass_ends(zz):
        @pl.when(z + 1 < n_z)
        def _():
            up_copy(zz).start()

        for h in range(1, n_x):
            side_copy(zz, h).start()

    def relay_ends(i):
        @pl.when(z >= i)
        def _():
            up_copy(z - i).wait_recv()
            pass_ends(z - i)

    def collect_ends(zz):
        @pl.when(z >= zz)
        def _():
            for h in range(1, n_x):
                side_copy(zz, h).wait_recv()

    def close_ends(zz):
        @pl.when(z >= zz)
        def _():
            @pl.when(z + 1 < n_z)
            def _():
                up_copy(zz).wait_send()

            for h in range(1, n_x):
                side_copy(zz, h).wait_send()

    def near_copy(b, h):
        at = pl.ds(b * half_rows, half_rows)
        src = part_ref.at[at, columns(2 * peer_y(h) + 1 - core)]
        return remote(src, near_ref.at[h, at, :], ns.at[b, h], nr.at[b, h], e, other)

    def back_copy(d, h):
        src = stage_ref.at[h, block(d), :]
        dst = far_ref.at[h, block(d), :]
        return remote(src, dst, bs.at[h, d], br.at[h, d], e, 2 * peer_y(h) + core)

    def home_copy(d):
        peer = lax.rem(e - d + n_ep, n_ep)
        return remote(
            final_ref.at[block(d), :], home_ref.at[block(e), :], hs.at[d], hr.at[d], peer, t
        )

    def pair_sum(d, h):
        return wide(part_ref[block(d), columns(2 * peer_y(h) + core)]) + wide(near_ref[h, block(d), :])

    def add_near(b):
        for h in range(n_y):
            near_copy(b, h).wait_recv()

        def one(d):
            for h in range(1, n_y):
                stage_ref[h, block(d), :] = bf(pair_sum(d, h))
                back_copy(d, h).start()

        span(b * half, (b + 1) * half, one)

    def add_far(d):
        total = pair_sum(d, 0)
        for h in range(1, n_y):
            back_copy(d, h).wait_recv()
            total = total + wide(far_ref[h, block(d), :])
        return bf(total)

    def go_home(d):
        final_ref[block(d), :] = add_far(d)
        home_copy(d).start()

    def row_block(index, q):
        return pl.ds(pl.multiple_of((2 * index + q) * rows, rows), rows)

    def mnear_copy(q, h):
        src = proj_ref.at[row_block(2 * peer_y(h) + 1 - core, q), :]
        return remote(src, mnear_ref.at[q, h], mns.at[q, h], mnr.at[q, h], e, other)

    def my_copy(q, h):
        target = 2 * peer_y(h) + core
        return remote(
            mstage_ref.at[q, h], mfar_ref.at[q, h], mys.at[q, h], myr.at[q, h], e, target
        )

    def mixer_sum(q, h):
        return wide(proj_ref[row_block(2 * peer_y(h) + core, q), :]) + wide(mnear_ref[q, h])

    def mixer_share(q):
        for h in range(1, n_y):
            mnear_copy(q, h).wait_recv()
            mstage_ref[q, h] = bf(mixer_sum(q, h))
            my_copy(q, h).start()

    def mixer_end(q):
        mnear_copy(q, 0).wait_recv()
        total = mixer_sum(q, 0)
        for h in range(1, n_y):
            my_copy(q, h).wait_recv()
            total = total + wide(mfar_ref[q, h])
        mixer_ref[q * rows : (q + 1) * rows] = bf(total)

    def project(i):
        at = pl.ds(pl.multiple_of(i * wide_model, wide_model), wide_model)
        proj_ref[:, at] = bf(mm(mixed_ref[...], out_weight_ref[:, at]))

    def widen(b):
        def unit_tile(i):
            at = pl.ds(pl.multiple_of(i * wide_units, wide_units), wide_units)
            rows_in = piece_ref[b * half_rows : (b + 1) * half_rows, :]
            gate_val = mm(rows_in, gate_ref[:, at])
            hidden_ref[:, at] = bf(gate_val * logistic(gate_val) * mm(rows_in, up_ref[:, at]))

        span(0, units // wide_units, unit_tile)

    def narrow(b):
        at = slice(b * half_rows, (b + 1) * half_rows)

        def tile(index):
            part_ref[at, columns(index)] = bf(mm(hidden_ref[...], down_ref[:, columns(index)]))

        def send(i):
            h = n_y - 1 - i
            tile(2 * peer_y(h) + 1 - core)
            near_copy(b, h).start()

        span(0, n_y, send)
        span(0, n_y, lambda i: tile(2 * i + core))

    for copy in loads:
        copy.start()
    for i in range(units // wide_units):
        for copy in gate_copy(i):
            copy.start()
    for i in range(model // wide_model):
        down_copy(i).start()
    everyone_here = meet()

    order = flag(iota((tokens, tokens), 0) < iota((tokens, tokens), 1))
    expert_rows = max(16, experts)
    own_routes = routes_ref[...]
    names = iota((expert_rows, tokens), 0)
    named = [own_routes[k : k + 1, :] == names for k in range(own_routes.shape[0])]
    match = functools.reduce(jnp.logical_or, named)
    rank = mm(bf(flag(match)), bf(order))
    rank = jnp.where(match, rank, -1.0)
    level = iota((capacity, tokens), 0).astype(jnp.float32)
    for j in range(experts):
        place_ref[j * capacity : (j + 1) * capacity] = bf(flag(level == rank[j : j + 1, :]))
    loads[0].wait()
    step_rows = 32
    for i in range(tokens // step_rows):
        at = slice(i * step_rows, (i + 1) * step_rows)
        xw = wide(x_ref[at])
        scale = lax.rsqrt(jnp.mean(xw * xw, axis=-1, keepdims=True) + norm_eps)
        normed_ref[at] = bf(xw * scale * norm_gain_ref[...])
    own = normed_ref[:, columns(t)]
    for i in range(2):
        at = slice(i * half_rows, (i + 1) * half_rows)
        cols_ref[at] = bf(mm(place_ref[at], own))
    everyone_here()
    span(1, n_ep, lambda d: ep_copy(d).start())
    for i in range(model // wide_model):
        at = slice(i * wide_model, (i + 1) * wide_model)
        piece_ref[:capacity, at] = bf(mm(place_ref[block(e), :], normed_ref[:, at]))

    for copy in loads[1:6]:
        copy.wait()
    events = 4 * (r_ref.shape[0] // (group * HEAD_DIM))
    per, lag = -(-n_ep // events), 3

    def pump(g, point):
        p = 4 * g + point
        span(jnp.maximum(p * per, 1), jnp.minimum((p + 1) * per, n_ep), arrived)
        q = p - lag
        span(jnp.maximum(q * per, 1), jnp.minimum((q + 1) * per, n_ep), pass_on)

    scan_kernel(
        group,
        pump,
        r_ref,
        k_ref,
        v_ref,
        d_ref,
        a_ref,
        d_off_ref,
        a_off_ref,
        extra_ref,
        out_ref,
        reach_ref,
        every_ref.at[e],
        chain_ref,
    )
    pass_ends(z)
    passed = max(1, min(n_ep, (events - lag) * per))
    early = max(passed, half)
    span(passed, early, pass_on)
    for i in range(units // wide_units):
        for copy in gate_copy(i):
            copy.wait()
    for i in range(model // wide_model):
        down_copy(i).wait()
    span(1, half, gathered)
    widen(0)
    span(early, n_ep, pass_on)
    span(1, min(2, n_z), relay_ends)
    narrow(0)
    span(min(2, n_z), min(3, n_z), relay_ends)
    span(half, n_ep, gathered)
    add_near(0)
    widen(1)
    span(min(3, n_z), n_z, relay_ends)
    narrow(1)
    span(0, n_z, collect_ends)
    loads[6].wait()
    loads[7].wait()
    add_near(1)
    join_kernel("ep", every_ref, out_ref, reach_ref, gate_in_ref, gain_ref, mixed_ref)
    span(0, model // wide_model, project)
    for q in range(2):
        for h in range(n_y):
            mnear_copy(q, h).start()
    span(1, half, go_home)
    mixer_share(0)
    mixer_share(1)
    span(half, n_ep, go_home)
    home_ref[block(e), :] = add_far(0)

    normed = normed_ref[...]
    group_logit = mm_nt(group_router_ref[...], normed)
    group_exp = jnp.exp(group_logit)
    group_prob = group_exp / jnp.sum(group_exp, axis=0, keepdims=True)
    expert_logit = mm_nt(expert_router_ref[...], normed)
    per_group = experts // groups
    first_of = iota((groups, tokens), 0) * per_group
    expert_names = iota((experts, tokens), 0)
    chosen, prob = [], []
    for k in range(2):
        route = own_routes[k : k + 1, :]
        chosen.append(
            jnp.sum(jnp.where(route == expert_names, expert_logit, 0.0), axis=0, keepdims=True)
        )
        inside = (route >= first_of) & (route < first_of + per_group)
        prob.append(jnp.sum(jnp.where(inside, group_prob, 0.0), axis=0, keepdims=True))
    weights = [prob[0] * logistic(chosen[0] - chosen[1]), prob[1] * logistic(chosen[1] - chosen[0])]
    weights = [jnp.transpose(jnp.broadcast_to(w, (128, tokens))) for w in weights]
    picks = []
    for k in range(2):
        parts = []
        for j in range(experts):
            at = slice(j * capacity, (j + 1) * capacity)
            parts.append(place_ref[at] * bf(flag(own_routes[k : k + 1, :] == j)))
        picks.append(jnp.concatenate(parts, axis=0))

    mixer_end(0)
    span(1, n_ep, lambda d: home_copy(d).wait_recv())
    back = home_ref[...]
    first, second = mm_tn(picks[0], back), mm_tn(picks[1], back)
    for i in range(share // 128):
        at = slice(i * 128, (i + 1) * 128)
        expert_ref[:, at] = bf(weights[0] * first[:, at] + weights[1] * second[:, at])
    mixer_end(1)

    def close(d):
        ep_copy(d).wait_send()
        core_copy(d).wait_send()
        home_copy(d).wait_send()
        for h in range(1, n_y):
            y_copy(d, h).wait_send()
            forward_copy(d, h).wait_send()

    span(1, n_ep, close)

    def close_back(d):
        for h in range(1, n_y):
            back_copy(d, h).wait_send()

    span(0, n_ep, close_back)
    for b in range(2):
        for h in range(n_y):
            near_copy(b, h).wait_send()
            mnear_copy(b, h).wait_send()
        for h in range(1, n_y):
            my_copy(b, h).wait_send()
    span(0, n_z, close_ends)


def local(
    receptance,
    key_matrix,
    value_matrix,
    decay_data_term,
    correction_rate_data,
    output_gate_input,
    decay_channel_offset,
    correction_rate_offset,
    extra_head_log_decay,
    head_norm_gain,
    mixer_output_weight,
    expert_layer_input,
    feedforward_norm_gain,
    group_router_weight,
    expert_router_weight,
    routes,
    expert_gate_weight,
    expert_up_weight,
    expert_down_weight,
):
    positions, own_width = receptance.shape
    pairs = -(-own_width // PAIR)
    width = pairs * PAIR

    def filled(x, columns=width):
        return x if x.shape[-1] == columns else jnp.pad(x, ((0, 0), (0, columns - x.shape[-1])))

    blocks = positions // HEAD_DIM
    group = 4 if blocks % 4 == 0 else 1
    n_ep, n_tp = lax.axis_size("ep"), lax.axis_size("tp")
    n_y = n_tp // 2
    n_x = 1
    while 4 * n_x * n_x <= n_ep:
        n_x = 2 * n_x
    tokens, model = expert_layer_input.shape
    capacity, share = 4 * tokens // n_ep, model // n_tp
    slots = n_ep * capacity
    units = expert_gate_weight.shape[2]
    rows = positions // n_tp
    out_weight = jnp.pad(mixer_output_weight, ((0, width - own_width), (0, 0)))

    def held(*shape):
        return pltpu.VMEM(shape, jnp.bfloat16)

    def sems(*shape):
        return pltpu.SemaphoreType.DMA(shape)

    in_vmem, in_hbm = pl.BlockSpec(memory_space=pltpu.VMEM), pl.BlockSpec(memory_space=pltpu.HBM)
    one, many = sems(n_ep), sems(n_y, n_ep)
    mixer_out, expert_out = pl.pallas_call(
        functools.partial(whole_kernel, group),
        out_shape=(
            jax.ShapeDtypeStruct((rows, model), jnp.bfloat16),
            jax.ShapeDtypeStruct((tokens, share), jnp.bfloat16),
        ),
        in_specs=[in_hbm] * 6
        + [in_vmem] * 4
        + [in_hbm] * 2
        + [in_vmem] * 4
        + [in_hbm] * 3,
        out_specs=[in_vmem] * 2,
        scratch_shapes=[held(positions, width)] * 6
        + [
            held(width, model),
            held(tokens, model),
            held(tokens, model),
            held(slots, tokens),
            held(slots, share),
            held(slots, model),
            pltpu.VMEM((positions, width), jnp.float32),
            held(positions, width),
            held(n_ep, pairs * 2 * HEAD_DIM, PAIR),
            pltpu.VMEM((pairs, 2 * PAIR, PAIR), jnp.float32),
            held(positions, width),
            held(positions, model),
            held(model, units),
            held(model, units),
            held(units, model),
            held(slots // 2, units),
            held(slots, model),
        ]
        + [held(n_y, slots, share)] * 3
        + [held(slots, share)] * 2
        + [held(2, n_y, rows // 2, model)] * 3
        + [sems(8)]
        + [sems(max(1, units // 256))] * 2
        + [sems(max(1, model // 512))]
        + [one] * 4
        + [many] * 4
        + [sems(n_ep // n_x)] * 2
        + [sems(n_x, n_ep // n_x)] * 2
        + [sems(2, n_y)] * 2
        + [many] * 2
        + [one] * 2
        + [sems(2, n_y)] * 4,
        compiler_params=pltpu.CompilerParams(
            collective_id=0, has_side_effects=True, vmem_limit_bytes=VMEM_LIMIT
        ),
    )(
        filled(receptance),
        filled(key_matrix),
        filled(value_matrix),
        filled(decay_data_term),
        filled(correction_rate_data),
        filled(output_gate_input),
        filled(decay_channel_offset[None]),
        filled(correction_rate_offset[None]),
        filled(extra_head_log_decay, 2 * pairs),
        filled(head_norm_gain[None]),
        out_weight,
        expert_layer_input,
        feedforward_norm_gain[None],
        group_router_weight.T,
        expert_router_weight.T,
        routes.T,
        expert_gate_weight,
        expert_up_weight,
        expert_down_weight,
    )
    return mixer_out, expert_out


def solution(mesh):
    in_specs = (
        P("ep", "tp"),
        P("ep", "tp"),
        P("ep", "tp"),
        P("ep", "tp"),
        P("ep", "tp"),
        P("ep", "tp"),
        P("tp"),
        P("tp"),
        P("ep", "tp"),
        P("tp"),
        P("tp", None),
        P("ep", None),
        P(),
        P(),
        P(),
        P("ep", None),
        P("ep", None, "tp"),
        P("ep", None, "tp"),
        P("ep", "tp", None),
    )
    out_specs = (P(("ep", "tp"), None), P("ep", "tp"))
    return jax.shard_map(local, mesh=mesh, in_specs=in_specs, out_specs=out_specs, check_vma=False)
```

time: 78.3 us -> 60.4 us (0.77)
  Pallas kernels: 65.3 us -> 54.5 us
  matrix products: 4.91 us -> 0 us
  other arithmetic: 2.87 us -> 0 us
  local copies, waits for them, and re-layouts: 3.74 us -> 5 us
    pallas_call x2 -> x1, Pallas kernels: 65.3 us -> 54.5 us  [local(): pl.pallas_call(functools.partial(whole_kernel, group), out_shape=(jax.Sha...]
    dot_general x4 -> x0, matrix products: 4.91 us -> none  [the longest x1 3.18 us: expert_route(): jnp.dot(dispatch_matrix, normed_input, preferred_element_type=jnp.float32)]
    unnamed x41 -> x3, local copies, waits for them, and re-layouts: 1.93 us -> 5 us
    reduce_sum x5 -> x0, other arithmetic: 1.45 us -> none  [the longest x1 1.23 us: expert_route(): jnp.mean(widened * widened, axis=-1, keepdims=True) + norm_eps]
    dynamic_slice x1 -> x0, local copies, waits for them, and re-layouts: 1.08 us -> none  [expert_route(): lax.dynamic_slice_in_dim(outgoing, lax.axis_index('tp') * width_share, wi...]
where the time goes in v1:
time: 60.4 us; the launch traced here: 60.2 us
  Pallas kernels  54.5 us (90%)
  local copies, waits for them, and re-layouts  5 us (8%)
  between operations  0.64 us (1%)
    pallas_call x1, Pallas kernels, local(): pl.pallas_call(functools.partial(whole_kernel, group), out_shape=(jax.Sha...  54.5 us
    unnamed x3, local copies, waits for them, and re-layouts  5 us

profile of v1, /device:TPU:0, one launch (start us, length us, event | category | flops | bytes accessed | tf_op | source)
XLA Modules:
  0.0 60.2 jit_solution(12985249522989183814)
XLA Ops:
  0.6 1.6 %copy.21.extra_ref = f32[512,4]{1,0:T(8,128)} copy(f32[512,4]{0,1:T(4,128)} %param.27) | data formatting | bytes 16384 | tf_op args[8]
  2.2 54.5 %shard_map.194 = (bf16[128,2048]{1,0:T(8,128)(2,1)}, bf16[128,512]{1,0:T(8,128)(2,1)}) custom-call(bf16[512,256]{1,0:T(8,128)(2,1)} %r_hbm.1, bf16[512,256]{1,0:T(8,128)(2,1)} %k_hbm.1, bf16[512,256]{1,0:T(8,128)(2,1)} %v_hbm.1, bf16[512,256]{1,0:T(8,128)(2,1)} %d_hbm.1, bf16[512,256]{1,0:T(8,128)(2,1)} %a_hbm.1, bf16[512,256]{1,0:T(8,128)(2,1)} %gate_in_hbm.1, ...), custom_call_target="tpu_custom_call" | custom-call | tf_op jit(solution)/shard_map/pallas_call | solution.py:786
  56.7 1.9 %copy.24 = bf16[128,2048]{1,0:T(8,128)(2,1)} copy(bf16[128,2048]{1,0:T(8,128)(2,1)} %get-tuple-element.4) | data formatting | bytes 1048576
  58.6 1.6 %copy.25 = bf16[128,512]{1,0:T(8,128)(2,1)} copy(bf16[128,512]{1,0:T(8,128)(2,1)} %get-tuple-element.5) | data formatting | bytes 262144

commit v2 on v1

--- a/solution.py
+++ b/solution.py
@@ -10,7 +10,7 @@
 
 HEAD_DIM = 64
 PAIR = 2 * HEAD_DIM
-VMEM_LIMIT = 56 << 20
+VMEM_LIMIT = 48 << 20
 HALF_EXP = math.exp(-0.5)
 GROUPS = 4
 
@@ -88,7 +88,6 @@
     row, col = iota((C, PAIR), 0), iota((C, PAIR), 1) & (HEAD_DIM - 1)
     strict, upto = row > col, row >= col
     eye = flag(row == col)
-    first = iota((1, PAIR), 1) < HEAD_DIM
     tri = bf(flag(iota((C, C), 0) >= iota((C, C), 1)))
     level_masks = []
     for s in range(6):
@@ -116,9 +115,7 @@
             k = k_ref[rows, lanes].astype(jnp.float32)
             u = k * lax.rsqrt(sum_right(k * k, own_bf) + key_eps)
             rem = u * logistic(a_ref[rows, lanes].astype(jnp.float32) + a_off_ref[:, lanes])
-            e = extra_ref[rows, :]
-            extra = jnp.where(first, e[:, 2 * p : 2 * p + 1], e[:, 2 * p + 1 : 2 * p + 2])
-            lg = extra - HALF_EXP * logistic(
+            lg = extra_ref[rows, lanes] - HALF_EXP * logistic(
                 d_ref[rows, lanes].astype(jnp.float32) + d_off_ref[:, lanes]
             )
             r = r_ref[rows, lanes].astype(jnp.float32)
@@ -287,16 +284,16 @@
     d_hbm,
     a_hbm,
     gate_in_hbm,
-    d_off_ref,
-    a_off_ref,
-    extra_ref,
-    gain_ref,
+    d_off_hbm,
+    a_off_hbm,
+    extra_hbm,
+    gain_hbm,
     out_weight_hbm,
     x_hbm,
-    norm_gain_ref,
-    group_router_ref,
-    expert_router_ref,
-    routes_ref,
+    norm_gain_hbm,
+    group_router_hbm,
+    expert_router_hbm,
+    routes_hbm,
     gate_hbm,
     up_hbm,
     down_hbm,
@@ -310,6 +307,16 @@
     gate_in_ref,
     out_weight_ref,
     x_ref,
+    d_off_ref,
+    a_off_ref,
+    extra_in_ref,
+    gain_ref,
+    norm_gain_ref,
+    group_router_ref,
+    expert_router_ref,
+    routes_ref,
+    extra_parts_ref,
+    extra_ref,
     normed_ref,
     place_ref,
     cols_ref,
@@ -369,15 +376,18 @@
     capacity = slots // n_ep
     experts = expert_router_ref.shape[0]
     groups = group_router_ref.shape[0]
-    rows = proj_ref.shape[0] // (2 * n_tp)
+    positions = proj_ref.shape[0]
+    rows = positions // n_tp
     other = 2 * y + 1 - core
     half = n_ep // 2
     half_rows = half * capacity
     wide_units, wide_model = min(256, units), min(512, model)
 
-    inputs = [(x_hbm, x_ref)]
+    inputs = [(routes_hbm, routes_ref), (norm_gain_hbm, norm_gain_ref), (x_hbm, x_ref)]
+    inputs += [(extra_hbm, extra_in_ref), (d_off_hbm, d_off_ref), (a_off_hbm, a_off_ref)]
     inputs += [(k_hbm, k_ref), (a_hbm, a_ref), (d_hbm, d_ref), (r_hbm, r_ref), (v_hbm, v_ref)]
-    inputs += [(gate_in_hbm, gate_in_ref), (out_weight_hbm, out_weight_ref)]
+    inputs += [(gate_in_hbm, gate_in_ref), (out_weight_hbm, out_weight_ref), (gain_hbm, gain_ref)]
+    inputs += [(group_router_hbm, group_router_ref), (expert_router_hbm, expert_router_ref)]
     loads = [pltpu.make_async_copy(s, d, in_sem.at[i]) for i, (s, d) in enumerate(inputs)]
 
     def gate_copy(i):
@@ -391,6 +401,13 @@
         at = pl.ds(pl.multiple_of(i * wide_model, wide_model), wide_model)
         return pltpu.make_async_copy(down_hbm.at[0, :, at], down_ref.at[:, at], down_sem.at[i])
 
+    def partner(d):
+        bit, total = 1, 0
+        while bit < n_ep:
+            total = total + lax.rem(lax.div(e, bit) + lax.div(d, bit), 2) * bit
+            bit = 2 * bit
+        return total
+
     def columns(index):
         return pl.ds(pl.multiple_of(index * share, share), share)
 
@@ -401,7 +418,7 @@
         return lax.rem(y + h, n_y)
 
     def ep_copy(d):
-        peer = lax.rem(e + d, n_ep)
+        peer = partner(d)
         return remote(
             cols_ref.at[block(peer), :], piece_ref.at[block(d), columns(t)], es.at[d], er.at[d], peer, t
         )
@@ -488,7 +505,7 @@
         return remote(src, dst, bs.at[h, d], br.at[h, d], e, 2 * peer_y(h) + core)
 
     def home_copy(d):
-        peer = lax.rem(e - d + n_ep, n_ep)
+        peer = partner(d)
         return remote(
             final_ref.at[block(d), :], home_ref.at[block(e), :], hs.at[d], hr.at[d], peer, t
         )
@@ -518,62 +535,81 @@
         final_ref[block(d), :] = add_far(d)
         home_copy(d).start()
 
-    def row_block(index, q):
-        return pl.ds(pl.multiple_of((2 * index + q) * rows, rows), rows)
-
-    def mnear_copy(q, h):
-        src = proj_ref.at[row_block(2 * peer_y(h) + 1 - core, q), :]
-        return remote(src, mnear_ref.at[q, h], mns.at[q, h], mnr.at[q, h], e, other)
-
-    def my_copy(q, h):
+    tile_count = model // wide_model
+
+    def tile_of(i):
+        return slice(i * wide_model, (i + 1) * wide_model)
+
+    def row_block(index):
+        return pl.ds(pl.multiple_of(index * rows, rows), rows)
+
+    def mnear_copy(i, h):
+        src = proj_ref.at[row_block(2 * peer_y(h) + 1 - core), tile_of(i)]
+        return remote(src, mnear_ref.at[i, h], mns.at[i, h], mnr.at[i, h], e, other)
+
+    def my_copy(i, h):
         target = 2 * peer_y(h) + core
         return remote(
-            mstage_ref.at[q, h], mfar_ref.at[q, h], mys.at[q, h], myr.at[q, h], e, target
+            mstage_ref.at[i, h], mfar_ref.at[i, h], mys.at[i, h], myr.at[i, h], e, target
         )
 
-    def mixer_sum(q, h):
-        return wide(proj_ref[row_block(2 * peer_y(h) + core, q), :]) + wide(mnear_ref[q, h])
-
-    def mixer_share(q):
+    def mixer_sum(i, h):
+        return wide(proj_ref[row_block(2 * peer_y(h) + core), tile_of(i)]) + wide(mnear_ref[i, h])
+
+    def project(i):
+        proj_ref[:, tile_of(i)] = bf(mm(mixed_ref[...], out_weight_ref[:, tile_of(i)]))
+        for h in range(n_y):
+            mnear_copy(i, h).start()
+
+    def mixer_share(i):
         for h in range(1, n_y):
-            mnear_copy(q, h).wait_recv()
-            mstage_ref[q, h] = bf(mixer_sum(q, h))
-            my_copy(q, h).start()
-
-    def mixer_end(q):
-        mnear_copy(q, 0).wait_recv()
-        total = mixer_sum(q, 0)
+            mnear_copy(i, h).wait_recv()
+            mstage_ref[i, h] = bf(mixer_sum(i, h))
+            my_copy(i, h).start()
+
+    def mixer_end(i):
+        mnear_copy(i, 0).wait_recv()
+        total = mixer_sum(i, 0)
         for h in range(1, n_y):
-            my_copy(q, h).wait_recv()
-            total = total + wide(mfar_ref[q, h])
-        mixer_ref[q * rows : (q + 1) * rows] = bf(total)
-
-    def project(i):
-        at = pl.ds(pl.multiple_of(i * wide_model, wide_model), wide_model)
-        proj_ref[:, at] = bf(mm(mixed_ref[...], out_weight_ref[:, at]))
-
-    def widen(b):
+            my_copy(i, h).wait_recv()
+            total = total + wide(mfar_ref[i, h])
+        mixer_ref[:, tile_of(i)] = bf(total)
+
+    def tiles(count, body, hooks):
+        for i in range(count):
+            body(i)
+            for hook in hooks.get(i, ()):
+                hook()
+        for i in sorted(hooks):
+            for hook in hooks[i] if i >= count else ():
+                hook()
+
+    def widen(b, hooks):
         def unit_tile(i):
-            at = pl.ds(pl.multiple_of(i * wide_units, wide_units), wide_units)
+            at = slice(i * wide_units, (i + 1) * wide_units)
+            if b == 0:
+                for copy in gate_copy(i):
+                    copy.wait()
             rows_in = piece_ref[b * half_rows : (b + 1) * half_rows, :]
             gate_val = mm(rows_in, gate_ref[:, at])
             hidden_ref[:, at] = bf(gate_val * logistic(gate_val) * mm(rows_in, up_ref[:, at]))
 
-        span(0, units // wide_units, unit_tile)
-
-    def narrow(b):
+        tiles(units // wide_units, unit_tile, hooks)
+
+    def narrow(b, hooks):
         at = slice(b * half_rows, (b + 1) * half_rows)
-
-        def tile(index):
+        if b == 0:
+            for i in range(tile_count):
+                down_copy(i).wait()
+
+        def tile(i):
+            h = n_y - 1 - i % n_y
+            index = 2 * peer_y(h) + (1 - core if i < n_y else core)
             part_ref[at, columns(index)] = bf(mm(hidden_ref[...], down_ref[:, columns(index)]))
-
-        def send(i):
-            h = n_y - 1 - i
-            tile(2 * peer_y(h) + 1 - core)
-            near_copy(b, h).start()
-
-        span(0, n_y, send)
-        span(0, n_y, lambda i: tile(2 * i + core))
+            if i < n_y:
+                near_copy(b, h).start()
+
+        tiles(n_tp, tile, hooks)
 
     for copy in loads:
         copy.start()
@@ -586,6 +622,8 @@
 
     order = flag(iota((tokens, tokens), 0) < iota((tokens, tokens), 1))
     expert_rows = max(16, experts)
+    loads[0].wait()
+    loads[1].wait()
     own_routes = routes_ref[...]
     names = iota((expert_rows, tokens), 0)
     named = [own_routes[k : k + 1, :] == names for k in range(own_routes.shape[0])]
@@ -595,7 +633,7 @@
     level = iota((capacity, tokens), 0).astype(jnp.float32)
     for j in range(experts):
         place_ref[j * capacity : (j + 1) * capacity] = bf(flag(level == rank[j : j + 1, :]))
-    loads[0].wait()
+    loads[2].wait()
     step_rows = 32
     for i in range(tokens // step_rows):
         at = slice(i * step_rows, (i + 1) * step_rows)
@@ -612,16 +650,47 @@
         at = slice(i * wide_model, (i + 1) * wide_model)
         piece_ref[:capacity, at] = bf(mm(place_ref[block(e), :], normed_ref[:, at]))
 
-    for copy in loads[1:6]:
+    for copy in loads[3:11]:
         copy.wait()
-    events = 4 * (r_ref.shape[0] // (group * HEAD_DIM))
-    per, lag = -(-n_ep // events), 3
+    heads, pairs = extra_in_ref.shape[0], chain_ref.shape[0]
+    exact = extra_in_ref[...]
+    extra_parts_ref[...] = jnp.zeros(extra_parts_ref.shape, jnp.float32)
+    for i in range(3):
+        piece = wide(bf(exact))
+        extra_parts_ref[i * heads : (i + 1) * heads, :] = piece
+        exact = exact - piece
+    extra_parts = bf(extra_parts_ref[...])
+    extra_rows = extra_parts_ref.shape[0]
+    for p in range(pairs):
+        head = lax.rem(iota((extra_rows, PAIR), 0), heads)
+        wanted = head == 2 * p + lax.div(iota((extra_rows, PAIR), 1), HEAD_DIM)
+        extra_ref[:, p * PAIR : (p + 1) * PAIR] = mm_tn(extra_parts, bf(flag(wanted)))
+    steps = positions // (group * HEAD_DIM)
+    per = max(1, n_ep // 8)
+
+    def unit(u, body):
+        lo = max(1, min(n_ep, u * per))
+        return lambda: span(lo, max(lo, min(n_ep, (u + 1) * per)), body)
+
+    events = {
+        1: [unit(0, arrived)],
+        2: [unit(1, arrived)],
+        3: [unit(2, arrived)],
+        4: [unit(3, arrived), unit(0, pass_on)],
+        5: [unit(1, pass_on)],
+        6: [unit(4, arrived), unit(2, pass_on)],
+        7: [unit(5, arrived), unit(3, pass_on)],
+    }
 
     def pump(g, point):
-        p = 4 * g + point
-        span(jnp.maximum(p * per, 1), jnp.minimum((p + 1) * per, n_ep), arrived)
-        q = p - lag
-        span(jnp.maximum(q * per, 1), jnp.minimum((q + 1) * per, n_ep), pass_on)
+        for step in range(steps):
+            due = events.get(4 * step + point)
+            if due:
+
+                @pl.when(g == step)
+                def _(due=due):
+                    for act in due:
+                        act()
 
     scan_kernel(
         group,
@@ -639,39 +708,37 @@
         every_ref.at[e],
         chain_ref,
     )
+    for i in sorted(events):
+        for act in events[i] if i >= 4 * steps else ():
+            act()
     pass_ends(z)
-    passed = max(1, min(n_ep, (events - lag) * per))
-    early = max(passed, half)
-    span(passed, early, pass_on)
-    for i in range(units // wide_units):
-        for copy in gate_copy(i):
-            copy.wait()
-    for i in range(model // wide_model):
-        down_copy(i).wait()
     span(1, half, gathered)
-    widen(0)
-    span(early, n_ep, pass_on)
-    span(1, min(2, n_z), relay_ends)
-    narrow(0)
-    span(min(2, n_z), min(3, n_z), relay_ends)
+    widen(0, {0: [unit(6, arrived)], 1: [unit(4, pass_on)], 2: [unit(7, arrived), unit(5, pass_on)]})
+    relay_ends(1) if n_z > 1 else None
+    narrow(0, {1: [unit(6, pass_on)]})
+    add_near(0)
+    unit(7, pass_on)()
     span(half, n_ep, gathered)
-    add_near(0)
-    widen(1)
-    span(min(3, n_z), n_z, relay_ends)
-    narrow(1)
+    relays = [lambda i=i: relay_ends(i) for i in range(2, n_z)]
+    widen(1, {1: relays[:1]})
+    narrow(1, {})
+    for relay in relays[1:]:
+        relay()
+    add_near(1)
+    span(1, half, go_home)
+    for copy in loads[11:]:
+        copy.wait()
     span(0, n_z, collect_ends)
-    loads[6].wait()
-    loads[7].wait()
-    add_near(1)
     join_kernel("ep", every_ref, out_ref, reach_ref, gate_in_ref, gain_ref, mixed_ref)
-    span(0, model // wide_model, project)
-    for q in range(2):
-        for h in range(n_y):
-            mnear_copy(q, h).start()
-    span(1, half, go_home)
-    mixer_share(0)
-    mixer_share(1)
-    span(half, n_ep, go_home)
+    homes = [unit(u, go_home) for u in range(4, 8)]
+    homes[0]()
+    for i in range(tile_count):
+        project(i)
+    homes[1]()
+    for i in range(tile_count):
+        mixer_share(i)
+    homes[2]()
+    homes[3]()
     home_ref[block(e), :] = add_far(0)
 
     normed = normed_ref[...]
@@ -700,14 +767,15 @@
             parts.append(place_ref[at] * bf(flag(own_routes[k : k + 1, :] == j)))
         picks.append(jnp.concatenate(parts, axis=0))
 
-    mixer_end(0)
+    for i in range(tile_count - 1):
+        mixer_end(i)
     span(1, n_ep, lambda d: home_copy(d).wait_recv())
     back = home_ref[...]
     first, second = mm_tn(picks[0], back), mm_tn(picks[1], back)
     for i in range(share // 128):
         at = slice(i * 128, (i + 1) * 128)
         expert_ref[:, at] = bf(weights[0] * first[:, at] + weights[1] * second[:, at])
-    mixer_end(1)
+    mixer_end(tile_count - 1)
 
     def close(d):
         ep_copy(d).wait_send()
@@ -727,9 +795,11 @@
     for b in range(2):
         for h in range(n_y):
             near_copy(b, h).wait_send()
-            mnear_copy(b, h).wait_send()
+    for i in range(tile_count):
+        for h in range(n_y):
+            mnear_copy(i, h).wait_send()
         for h in range(1, n_y):
-            my_copy(b, h).wait_send()
+            my_copy(i, h).wait_send()
     span(0, n_z, close_ends)
 
 
@@ -773,40 +843,68 @@
     slots = n_ep * capacity
     units = expert_gate_weight.shape[2]
     rows = positions // n_tp
+    tile_count = max(1, model // 512)
     out_weight = jnp.pad(mixer_output_weight, ((0, width - own_width), (0, 0)))
 
     def held(*shape):
         return pltpu.VMEM(shape, jnp.bfloat16)
 
+    def single(*shape):
+        return pltpu.VMEM(shape, jnp.float32)
+
     def sems(*shape):
         return pltpu.SemaphoreType.DMA(shape)
 
+    operands = (
+        filled(receptance),
+        filled(key_matrix),
+        filled(value_matrix),
+        filled(decay_data_term),
+        filled(correction_rate_data),
+        filled(output_gate_input),
+        filled(decay_channel_offset[None]),
+        filled(correction_rate_offset[None]),
+        filled(extra_head_log_decay, 2 * pairs).T,
+        filled(head_norm_gain[None]),
+        out_weight,
+        expert_layer_input,
+        feedforward_norm_gain[None],
+        group_router_weight.T,
+        expert_router_weight.T,
+        routes.T,
+        expert_gate_weight,
+        expert_up_weight,
+        expert_down_weight,
+    )
     in_vmem, in_hbm = pl.BlockSpec(memory_space=pltpu.VMEM), pl.BlockSpec(memory_space=pltpu.HBM)
     one, many = sems(n_ep), sems(n_y, n_ep)
     mixer_out, expert_out = pl.pallas_call(
         functools.partial(whole_kernel, group),
-        out_shape=(
-            jax.ShapeDtypeStruct((rows, model), jnp.bfloat16),
-            jax.ShapeDtypeStruct((tokens, share), jnp.bfloat16),
-        ),
-        in_specs=[in_hbm] * 6
-        + [in_vmem] * 4
-        + [in_hbm] * 2
-        + [in_vmem] * 4
-        + [in_hbm] * 3,
+        out_shape=(held(rows, model), held(tokens, share)),
+        in_specs=[in_hbm] * 19,
         out_specs=[in_vmem] * 2,
         scratch_shapes=[held(positions, width)] * 6
         + [
             held(width, model),
             held(tokens, model),
+            single(1, width),
+            single(1, width),
+            single(2 * pairs, positions),
+            single(1, width),
+            single(1, model),
+            held(*group_router_weight.shape[::-1]),
+            held(*expert_router_weight.shape[::-1]),
+            pltpu.VMEM(routes.shape[::-1], jnp.int32),
+            single(16, positions),
+            single(positions, width),
             held(tokens, model),
             held(slots, tokens),
             held(slots, share),
             held(slots, model),
-            pltpu.VMEM((positions, width), jnp.float32),
+            single(positions, width),
             held(positions, width),
             held(n_ep, pairs * 2 * HEAD_DIM, PAIR),
-            pltpu.VMEM((pairs, 2 * PAIR, PAIR), jnp.float32),
+            single(pairs, 2 * PAIR, PAIR),
             held(positions, width),
             held(positions, model),
             held(model, units),
@@ -817,8 +915,8 @@
         ]
         + [held(n_y, slots, share)] * 3
         + [held(slots, share)] * 2
-        + [held(2, n_y, rows // 2, model)] * 3
-        + [sems(8)]
+        + [held(tile_count, n_y, rows, model // tile_count)] * 3
+        + [sems(16)]
         + [sems(max(1, units // 256))] * 2
         + [sems(max(1, model // 512))]
         + [one] * 4
@@ -828,30 +926,12 @@
         + [sems(2, n_y)] * 2
         + [many] * 2
         + [one] * 2
-        + [sems(2, n_y)] * 4,
+        + [sems(tile_count, n_y)] * 4,
         compiler_params=pltpu.CompilerParams(
             collective_id=0, has_side_effects=True, vmem_limit_bytes=VMEM_LIMIT
         ),
     )(
-        filled(receptance),
-        filled(key_matrix),
-        filled(value_matrix),
-        filled(decay_data_term),
-        filled(correction_rate_data),
-        filled(output_gate_input),
-        filled(decay_channel_offset[None]),
-        filled(correction_rate_offset[None]),
-        filled(extra_head_log_decay, 2 * pairs),
-        filled(head_norm_gain[None]),
-        out_weight,
-        expert_layer_input,
-        feedforward_norm_gain[None],
-        group_router_weight.T,
-        expert_router_weight.T,
-        routes.T,
-        expert_gate_weight,
-        expert_up_weight,
-        expert_down_weight,
+        *(pltpu.with_memory_space_constraint(x, pltpu.HBM) for x in operands)
     )
     return mixer_out, expert_out
 

time: 60.4 us -> 52.5 us (0.87)
  Pallas kernels: 54.5 us -> 49.9 us
  local copies, waits for them, and re-layouts: 5 us -> 1.45 us
    pallas_call x1, Pallas kernels: 54.5 us -> 49.9 us  [local(): pl.pallas_call(functools.partial(whole_kernel, group), out_shape=(held(ro...]
    unnamed x3 -> x2, local copies, waits for them, and re-layouts: 5 us -> 1.45 us
where the time goes in v2:
time: 52.5 us; the launch traced here: 52 us
  Pallas kernels  49.9 us (95%)
  local copies, waits for them, and re-layouts  1.45 us (3%)
  between operations  0.65 us (1%)
    pallas_call x1, Pallas kernels, local(): pl.pallas_call(functools.partial(whole_kernel, group), out_shape=(held(ro...  49.9 us
    unnamed x2, local copies, waits for them, and re-layouts  1.45 us

profile of v2, /device:TPU:0, one launch (start us, length us, event | category | flops | bytes accessed | tf_op | source)
XLA Modules:
  0.0 52.0 jit_solution(5794477101858822174)
XLA Ops:
  0.6 49.9 %shard_map.194 = (bf16[128,2048]{1,0:T(8,128)(2,1)S(1)}, bf16[128,512]{1,0:T(8,128)(2,1)S(1)}) custom-call(bf16[512,256]{1,0:T(8,128)(2,1)} %r_hbm.1, bf16[512,256]{1,0:T(8,128)(2,1)} %k_hbm.1, bf16[512,256]{1,0:T(8,128)(2,1)} %v_hbm.1, bf16[512,256]{1,0:T(8,128)(2,1)} %d_hbm.1, bf16[512,256]{1,0:T(8,128)(2,1)} %a_hbm.1, bf16[512,256]{1,0:T(8,128)(2,1)} %gate_in_hbm.1, ...), custom_call_target="tpu_custom_call" | custom-call | tf_op jit(solution)/shard_map/pallas_call | solution.py:881
  50.6 0.8 %copy.23 = bf16[128,2048]{1,0:T(8,128)(2,1)} copy(bf16[128,2048]{1,0:T(8,128)(2,1)S(1)} %get-tuple-element.2) | data formatting | bytes 1048576
  51.4 0.7 %copy.24 = bf16[128,512]{1,0:T(8,128)(2,1)} copy(bf16[128,512]{1,0:T(8,128)(2,1)S(1)} %get-tuple-element.3) | data formatting | bytes 262144

commit v3 on v2

--- a/solution.py
+++ b/solution.py
@@ -261,7 +261,8 @@
     greet(e, 2 * y + 1 - core)
     for d in range(1, n_y):
         greet(e, 2 * lax.rem(y + d, n_y) + core)
-    return lambda: pl.semaphore_wait(barrier, n_ep - 1 + n_y)
+        greet(e, 2 * lax.rem(y + d, n_y) + 1 - core)
+    return lambda: pl.semaphore_wait(barrier, n_ep - 2 + 2 * n_y)
 
 
 def span(first, last, body):
@@ -305,7 +306,7 @@
     d_ref,
     a_ref,
     gate_in_ref,
-    out_weight_ref,
+    w_ref,
     x_ref,
     d_off_ref,
     a_off_ref,
@@ -319,27 +320,29 @@
     extra_ref,
     normed_ref,
     place_ref,
-    cols_ref,
+    near_out_ref,
+    far_out_ref,
+    picks_ref,
+    weight_ref,
     piece_ref,
     out_ref,
     reach_ref,
     every_ref,
     chain_ref,
     mixed_ref,
-    proj_ref,
+    mixed_all_ref,
     gate_ref,
     up_ref,
     down_ref,
     hidden_ref,
+    gate_part_ref,
+    up_part_ref,
     part_ref,
     near_ref,
     stage_ref,
     far_ref,
     final_ref,
     home_ref,
-    mnear_ref,
-    mstage_ref,
-    mfar_ref,
     in_sem,
     gate_sem,
     up_sem,
@@ -362,10 +365,14 @@
     br,
     hs,
     hr,
-    mns,
-    mnr,
-    mys,
-    myr,
+    wys,
+    wyr,
+    wgs,
+    wgr,
+    wcs,
+    wcr,
+    xs,
+    xr,
 ):
     n_ep, n_tp, n_y, e, t, y, core = place_of()
     units = gate_ref.shape[1]
@@ -376,30 +383,33 @@
     capacity = slots // n_ep
     experts = expert_router_ref.shape[0]
     groups = group_router_ref.shape[0]
-    positions = proj_ref.shape[0]
+    positions, width = mixed_ref.shape
     rows = positions // n_tp
     other = 2 * y + 1 - core
     half = n_ep // 2
     half_rows = half * capacity
     wide_units, wide_model = min(256, units), min(512, model)
 
+    def shard(index):
+        return pl.ds(pl.multiple_of(index * width, width), width)
+
     inputs = [(routes_hbm, routes_ref), (norm_gain_hbm, norm_gain_ref), (x_hbm, x_ref)]
     inputs += [(extra_hbm, extra_in_ref), (d_off_hbm, d_off_ref), (a_off_hbm, a_off_ref)]
     inputs += [(k_hbm, k_ref), (a_hbm, a_ref), (d_hbm, d_ref), (r_hbm, r_ref), (v_hbm, v_ref)]
-    inputs += [(gate_in_hbm, gate_in_ref), (out_weight_hbm, out_weight_ref), (gain_hbm, gain_ref)]
+    inputs += [(gate_in_hbm, gate_in_ref), (out_weight_hbm, w_ref.at[shard(t), :]), (gain_hbm, gain_ref)]
     inputs += [(group_router_hbm, group_router_ref), (expert_router_hbm, expert_router_ref)]
     loads = [pltpu.make_async_copy(s, d, in_sem.at[i]) for i, (s, d) in enumerate(inputs)]
 
     def gate_copy(i):
         at = pl.ds(pl.multiple_of(i * wide_units, wide_units), wide_units)
         return (
-            pltpu.make_async_copy(gate_hbm.at[0, :, at], gate_ref.at[:, at], gate_sem.at[i]),
-            pltpu.make_async_copy(up_hbm.at[0, :, at], up_ref.at[:, at], up_sem.at[i]),
+            pltpu.make_async_copy(gate_hbm.at[0, :, at], gate_ref.at[:, at], gate_sem.at[0]),
+            pltpu.make_async_copy(up_hbm.at[0, :, at], up_ref.at[:, at], up_sem.at[0]),
         )
 
     def down_copy(i):
         at = pl.ds(pl.multiple_of(i * wide_model, wide_model), wide_model)
-        return pltpu.make_async_copy(down_hbm.at[0, :, at], down_ref.at[:, at], down_sem.at[i])
+        return pltpu.make_async_copy(down_hbm.at[0, :, at], down_ref.at[:, at], down_sem.at[0])
 
     def partner(d):
         bit, total = 1, 0
@@ -417,41 +427,55 @@
     def peer_y(h):
         return lax.rem(y + h, n_y)
 
-    def ep_copy(d):
-        peer = partner(d)
-        return remote(
-            cols_ref.at[block(peer), :], piece_ref.at[block(d), columns(t)], es.at[d], er.at[d], peer, t
-        )
-
-    def core_copy(d):
-        ref = piece_ref.at[block(d), columns(t)]
-        return remote(ref, ref, cs.at[d], cr.at[d], e, other)
+    plane = pl.ds(pl.multiple_of(core * (model // 2), model // 2), model // 2)
+
+    def near_ep(d):
+        dst = piece_ref.at[block(d), plane]
+        return remote(near_out_ref.at[block(d), :], dst, es.at[0], er.at[d], partner(d), t)
+
+    def far_ep(d):
+        src = far_out_ref.at[block(d - half), :]
+        return remote(src, piece_ref.at[block(d), columns(t)], es.at[1], er.at[d], partner(d), t)
+
+    near_rows, far_rows = slice(capacity, half_rows), slice(half_rows, slots)
+
+    def near_core(at):
+        ref = piece_ref.at[at, plane]
+        return remote(ref, ref, cs.at[0], cr.at[0], e, other)
+
+    def far_core(at):
+        ref = piece_ref.at[at, columns(t)]
+        return remote(ref, ref, cs.at[1], cr.at[1], e, other)
 
     def y_copy(d, h):
         ref = piece_ref.at[block(d), columns(t)]
-        return remote(ref, ref, ys.at[h, d], yr.at[h, d], e, 2 * peer_y(h) + core)
-
-    def forward_copy(d, h):
-        ref = piece_ref.at[block(d), columns(2 * lax.rem(y - h + n_y, n_y) + core)]
-        return remote(ref, ref, fs.at[h, d], fr.at[h, d], e, other)
-
-    def arrived(d):
-        ep_copy(d).wait_recv()
+        peer = 2 * peer_y(h) + core
+        return remote(ref, ref, ys.at[h - 1], yr.at[h - 1, d - half], e, peer)
+
+    def forward_copy(at, h):
+        ref = piece_ref.at[at, columns(2 * lax.rem(y - h + n_y, n_y) + core)]
+        return remote(ref, ref, fs.at[h - 1], fr.at[h - 1], e, other)
+
+    def near_arrived(d):
+        near_ep(d).wait_recv()
+        near_core(block(d)).start()
+
+    def far_arrived(d):
+        far_ep(d).wait_recv()
         for h in range(1, n_y):
             y_copy(d, h).start()
-        core_copy(d).start()
+        far_core(block(d)).start()
 
     def pass_on(d):
         for h in range(1, n_y):
             y_copy(d, h).wait_recv()
-            forward_copy(d, h).start()
-
-    def gathered(d):
-        core_copy(d).wait_recv()
+            forward_copy(block(d), h).start()
+
+    def gathered():
         for h in range(1, n_y):
-            forward_copy(d, h).wait_recv()
-
-    n_x = gs.shape[0]
+            forward_copy(far_rows, h).wait_recv()
+
+    n_x = gs.shape[0] + 1
     n_z = n_ep // n_x
     z, x = lax.div(e, n_x), lax.rem(e, n_x)
 
@@ -462,7 +486,7 @@
     def side_copy(zz, h):
         ref = every_ref.at[zz * n_x + x]
         peer = z * n_x + lax.rem(x + h, n_x)
-        return remote(ref, ref, gs.at[h, zz], gr.at[h, zz], peer, t)
+        return remote(ref, ref, gs.at[h - 1, zz], gr.at[h - 1, zz], peer, t)
 
     def pass_ends(zz):
         @pl.when(z + 1 < n_z)
@@ -472,8 +496,8 @@
         for h in range(1, n_x):
             side_copy(zz, h).start()
 
-    def relay_ends(i):
-        @pl.when(z >= i)
+    def relay_ends(i, wanted=True):
+        @pl.when((z >= i) & wanted)
         def _():
             up_copy(z - i).wait_recv()
             pass_ends(z - i)
@@ -497,24 +521,26 @@
     def near_copy(b, h):
         at = pl.ds(b * half_rows, half_rows)
         src = part_ref.at[at, columns(2 * peer_y(h) + 1 - core)]
-        return remote(src, near_ref.at[h, at, :], ns.at[b, h], nr.at[b, h], e, other)
+        return remote(src, near_ref.at[h, at, :], ns.at[0], nr.at[b, h], e, other)
 
     def back_copy(d, h):
         src = stage_ref.at[h, block(d), :]
         dst = far_ref.at[h, block(d), :]
-        return remote(src, dst, bs.at[h, d], br.at[h, d], e, 2 * peer_y(h) + core)
+        return remote(src, dst, bs.at[h - 1], br.at[h - 1, d], e, 2 * peer_y(h) + core)
 
     def home_copy(d):
-        peer = partner(d)
-        return remote(
-            final_ref.at[block(d), :], home_ref.at[block(e), :], hs.at[d], hr.at[d], peer, t
-        )
+        src, dst = final_ref.at[block(d), :], home_ref.at[block(e), :]
+        return remote(src, dst, hs.at[0], hr.at[0], partner(d), t)
+
+    def all_home():
+        src, dst = final_ref.at[capacity:, :], home_ref.at[capacity:, :]
+        return remote(src, dst, hs.at[0], hr.at[0], partner(1), t)
 
     def pair_sum(d, h):
         return wide(part_ref[block(d), columns(2 * peer_y(h) + core)]) + wide(near_ref[h, block(d), :])
 
     def add_near(b):
-        for h in range(n_y):
+        for h in range(1, n_y):
             near_copy(b, h).wait_recv()
 
         def one(d):
@@ -536,44 +562,44 @@
         home_copy(d).start()
 
     tile_count = model // wide_model
-
-    def tile_of(i):
-        return slice(i * wide_model, (i + 1) * wide_model)
-
-    def row_block(index):
-        return pl.ds(pl.multiple_of(index * rows, rows), rows)
-
-    def mnear_copy(i, h):
-        src = proj_ref.at[row_block(2 * peer_y(h) + 1 - core), tile_of(i)]
-        return remote(src, mnear_ref.at[i, h], mns.at[i, h], mnr.at[i, h], e, other)
-
-    def my_copy(i, h):
-        target = 2 * peer_y(h) + core
-        return remote(
-            mstage_ref.at[i, h], mfar_ref.at[i, h], mys.at[i, h], myr.at[i, h], e, target
-        )
-
-    def mixer_sum(i, h):
-        return wide(proj_ref[row_block(2 * peer_y(h) + core), tile_of(i)]) + wide(mnear_ref[i, h])
-
-    def project(i):
-        proj_ref[:, tile_of(i)] = bf(mm(mixed_ref[...], out_weight_ref[:, tile_of(i)]))
-        for h in range(n_y):
-            mnear_copy(i, h).start()
-
-    def mixer_share(i):
+    part_rows = width // half
+    part_at = lax.rem(e, half)
+
+    def source_of(h):
+        return 2 * lax.rem(y - h + n_y, n_y) + core
+
+    def shard_part(index):
+        return pl.ds(pl.multiple_of(index * width + part_at * part_rows, part_rows), part_rows)
+
+    def w_plane(h):
+        ref = w_ref.at[shard_part(t), :]
+        return remote(ref, ref, wys.at[h - 1], wyr.at[h - 1], e, 2 * peer_y(h) + core)
+
+    def w_group(h, k):
+        ref = w_ref.at[shard_part(source_of(h)), :]
+        return remote(ref, ref, wgs.at[0], wgr.at[0], partner(k), t)
+
+    def w_grouped():
+        ref = w_ref.at[: (n_y - 1) * (half - 1) * part_rows, :]
+        return remote(ref, ref, wgs.at[0], wgr.at[0], partner(1), t)
+
+    def w_core(h):
+        ref = w_ref.at[shard(source_of(h)), :]
+        return remote(ref, ref, wcs.at[h], wcr.at[h], e, other)
+
+    def share_w():
         for h in range(1, n_y):
-            mnear_copy(i, h).wait_recv()
-            mstage_ref[i, h] = bf(mixer_sum(i, h))
-            my_copy(i, h).start()
-
-    def mixer_end(i):
-        mnear_copy(i, 0).wait_recv()
-        total = mixer_sum(i, 0)
-        for h in range(1, n_y):
-            my_copy(i, h).wait_recv()
-            total = total + wide(mfar_ref[i, h])
-        mixer_ref[:, tile_of(i)] = bf(total)
+            w_plane(h).wait_recv()
+            span(1, half, lambda k: w_group(h, k).start())
+
+    def mixed_copy(j):
+        to = lax.rem(t + j, n_tp)
+        src = mixed_ref.at[pl.ds(pl.multiple_of(to * rows, rows), rows), :]
+        return remote(src, mixed_all_ref.at[t], xs.at[0], xr.at[0], e, to)
+
+    def all_mixed():
+        ref = mixed_all_ref.at[1:]
+        return remote(ref, ref, xs.at[0], xr.at[0], e, other)
 
     def tiles(count, body, hooks):
         for i in range(count):
@@ -584,23 +610,45 @@
             for hook in hooks[i] if i >= count else ():
                 hook()
 
-    def widen(b, hooks):
+    def units_at(i):
+        return slice(i * wide_units, (i + 1) * wide_units)
+
+    def activate(i, gate_val, up_val):
+        hidden_ref[:, units_at(i)] = bf(gate_val * logistic(gate_val) * up_val)
+
+    def widen_near(hooks):
+        pltpu.make_async_copy(gate_hbm.at[0], gate_ref, gate_sem.at[0]).wait()
+        pltpu.make_async_copy(up_hbm.at[0], up_ref, up_sem.at[0]).wait()
+
         def unit_tile(i):
-            at = slice(i * wide_units, (i + 1) * wide_units)
-            if b == 0:
-                for copy in gate_copy(i):
-                    copy.wait()
-            rows_in = piece_ref[b * half_rows : (b + 1) * half_rows, :]
-            gate_val = mm(rows_in, gate_ref[:, at])
-            hidden_ref[:, at] = bf(gate_val * logistic(gate_val) * mm(rows_in, up_ref[:, at]))
+            rows_in = piece_ref[:half_rows, :]
+            activate(i, mm(rows_in, gate_ref[:, units_at(i)]), mm(rows_in, up_ref[:, units_at(i)]))
+
+        tiles(units // wide_units, unit_tile, hooks)
+
+    def widen_part(i, h):
+        model_at = pl.ds(pl.multiple_of(peer_y(h) * 2 * share, 2 * share), 2 * share)
+        rows_in = piece_ref[far_rows, model_at]
+        return mm(rows_in, gate_ref[model_at, units_at(i)]), mm(rows_in, up_ref[model_at, units_at(i)])
+
+    def widen_far_begin():
+        for i in range(units // wide_units):
+            gate_part_ref[:, units_at(i)], up_part_ref[:, units_at(i)] = widen_part(i, 0)
+
+    def widen_far_end(hooks):
+        def unit_tile(i):
+            gate_val, up_val = gate_part_ref[:, units_at(i)], up_part_ref[:, units_at(i)]
+            for h in range(1, n_y):
+                more = widen_part(i, h)
+                gate_val, up_val = gate_val + more[0], up_val + more[1]
+            activate(i, gate_val, up_val)
 
         tiles(units // wide_units, unit_tile, hooks)
 
     def narrow(b, hooks):
         at = slice(b * half_rows, (b + 1) * half_rows)
         if b == 0:
-            for i in range(tile_count):
-                down_copy(i).wait()
+            pltpu.make_async_copy(down_hbm.at[0], down_ref, down_sem.at[0]).wait()
 
         def tile(i):
             h = n_y - 1 - i % n_y
@@ -640,16 +688,34 @@
         xw = wide(x_ref[at])
         scale = lax.rsqrt(jnp.mean(xw * xw, axis=-1, keepdims=True) + norm_eps)
         normed_ref[at] = bf(xw * scale * norm_gain_ref[...])
-    own = normed_ref[:, columns(t)]
-    for i in range(2):
-        at = slice(i * half_rows, (i + 1) * half_rows)
-        cols_ref[at] = bf(mm(place_ref[at], own))
+    here = jnp.concatenate([place_ref[block(partner(d)), :] for d in range(1, half)], axis=0)
+    near_out_ref[capacity:half_rows] = bf(mm(here, normed_ref[:, plane]))
+    there = jnp.concatenate([place_ref[block(partner(d)), :] for d in range(half, n_ep)], axis=0)
+    far_out_ref[...] = bf(mm(there, normed_ref[:, columns(t)]))
+    per = max(1, n_ep // 8)
+
+    def unit(u, body):
+        lo = max(1, min(n_ep, u * per))
+        return lambda: span(lo, max(lo, min(n_ep, (u + 1) * per)), body)
+
+    inner = lax.rem(lax.div(z + 1, 2), 2)
+
+    def far_unit(k, body):
+        first = [4 + 2 * inner, 5 + 2 * inner, 6 - 2 * inner, 7 - 2 * inner][k] * per
+        return lambda: span(first, first + per, body)
+
     everyone_here()
-    span(1, n_ep, lambda d: ep_copy(d).start())
+    span(1, half, lambda d: near_ep(d).start())
+    for k in range(4):
+        far_unit(k, lambda d: far_ep(d).start())()
     for i in range(model // wide_model):
         at = slice(i * wide_model, (i + 1) * wide_model)
         piece_ref[:capacity, at] = bf(mm(place_ref[block(e), :], normed_ref[:, at]))
 
+    loads[12].wait()
+    for h in range(1, n_y):
+        w_plane(h).start()
+    w_core(0).start()
     for copy in loads[3:11]:
         copy.wait()
     heads, pairs = extra_in_ref.shape[0], chain_ref.shape[0]
@@ -666,21 +732,7 @@
         wanted = head == 2 * p + lax.div(iota((extra_rows, PAIR), 1), HEAD_DIM)
         extra_ref[:, p * PAIR : (p + 1) * PAIR] = mm_tn(extra_parts, bf(flag(wanted)))
     steps = positions // (group * HEAD_DIM)
-    per = max(1, n_ep // 8)
-
-    def unit(u, body):
-        lo = max(1, min(n_ep, u * per))
-        return lambda: span(lo, max(lo, min(n_ep, (u + 1) * per)), body)
-
-    events = {
-        1: [unit(0, arrived)],
-        2: [unit(1, arrived)],
-        3: [unit(2, arrived)],
-        4: [unit(3, arrived), unit(0, pass_on)],
-        5: [unit(1, pass_on)],
-        6: [unit(4, arrived), unit(2, pass_on)],
-        7: [unit(5, arrived), unit(3, pass_on)],
-    }
+    events = {}
 
     def pump(g, point):
         for step in range(steps):
@@ -712,34 +764,17 @@
         for act in events[i] if i >= 4 * steps else ():
             act()
     pass_ends(z)
-    span(1, half, gathered)
-    widen(0, {0: [unit(6, arrived)], 1: [unit(4, pass_on)], 2: [unit(7, arrived), unit(5, pass_on)]})
-    relay_ends(1) if n_z > 1 else None
-    narrow(0, {1: [unit(6, pass_on)]})
+    span(1, half, near_arrived)
+    far_unit(0, far_arrived)()
+    far_unit(1, far_arrived)()
+    share_w()
+    near_core(near_rows).wait_recv()
+    relays = [lambda i=i: relay_ends(i) for i in range(1, n_z)]
+    widen_near({2: [far_unit(2, far_arrived)], 3: [far_unit(0, pass_on)]})
+    narrow(0, {0: [far_unit(1, pass_on)], 1: [far_unit(3, far_arrived)], 3: [far_unit(2, pass_on)]})
     add_near(0)
-    unit(7, pass_on)()
-    span(half, n_ep, gathered)
-    relays = [lambda i=i: relay_ends(i) for i in range(2, n_z)]
-    widen(1, {1: relays[:1]})
-    narrow(1, {})
-    for relay in relays[1:]:
-        relay()
-    add_near(1)
-    span(1, half, go_home)
-    for copy in loads[11:]:
+    for copy in loads[11:12] + loads[13:]:
         copy.wait()
-    span(0, n_z, collect_ends)
-    join_kernel("ep", every_ref, out_ref, reach_ref, gate_in_ref, gain_ref, mixed_ref)
-    homes = [unit(u, go_home) for u in range(4, 8)]
-    homes[0]()
-    for i in range(tile_count):
-        project(i)
-    homes[1]()
-    for i in range(tile_count):
-        mixer_share(i)
-    homes[2]()
-    homes[3]()
-    home_ref[block(e), :] = add_far(0)
 
     normed = normed_ref[...]
     group_logit = mm_nt(group_router_ref[...], normed)
@@ -758,49 +793,76 @@
         inside = (route >= first_of) & (route < first_of + per_group)
         prob.append(jnp.sum(jnp.where(inside, group_prob, 0.0), axis=0, keepdims=True))
     weights = [prob[0] * logistic(chosen[0] - chosen[1]), prob[1] * logistic(chosen[1] - chosen[0])]
-    weights = [jnp.transpose(jnp.broadcast_to(w, (128, tokens))) for w in weights]
-    picks = []
     for k in range(2):
-        parts = []
+        weight_ref[k] = jnp.transpose(jnp.broadcast_to(weights[k], (128, tokens)))
         for j in range(experts):
             at = slice(j * capacity, (j + 1) * capacity)
-            parts.append(place_ref[at] * bf(flag(own_routes[k : k + 1, :] == j)))
-        picks.append(jnp.concatenate(parts, axis=0))
-
-    for i in range(tile_count - 1):
-        mixer_end(i)
-    span(1, n_ep, lambda d: home_copy(d).wait_recv())
+            picks_ref[k, at] = place_ref[at] * bf(flag(own_routes[k : k + 1, :] == j))
+    far_core(far_rows).wait_recv()
+    widen_far_begin()
+    for relay in relays[:1]:
+        relay()
+    with jax.named_scope("pass3"):
+        far_unit(3, pass_on)()
+    near_copy(0, 0).wait_recv()
+    gathered()
+    last = z == n_z - 1
+    widen_far_end({1: [lambda i=i: relay_ends(i, ~last) for i in range(2, 3)]})
+    narrow(1, {})
+    add_near(1)
+    span(1, half, go_home)
+    near_copy(1, 0).wait_recv()
+    unit(4, go_home)()
+    for i in range(2, n_z):
+        relay_ends(i, last if i < 3 else True)
+    for u in range(5, 8):
+        unit(u, go_home)()
+    home_ref[block(e), :] = add_far(0)
+    span(0, n_z, collect_ends)
+    join_kernel("ep", every_ref, out_ref, reach_ref, gate_in_ref, gain_ref, mixed_ref)
+    for j in range(1, n_tp):
+        mixed_copy(j).start()
+    mixed_all_ref[t] = mixed_ref[pl.ds(pl.multiple_of(t * rows, rows), rows), :]
+    w_grouped().wait_recv()
+    for h in range(1, n_y):
+        w_core(h).start()
+    all_mixed().wait_recv()
+    for h in range(n_y):
+        w_core(h).wait_recv()
+    mixed = jnp.concatenate([mixed_all_ref[j] for j in range(n_tp)], axis=1)
+
+    def project(i):
+        at = pl.ds(pl.multiple_of(i * wide_model, wide_model), wide_model)
+        mixer_ref[:, at] = bf(mm(mixed, w_ref[:, at]))
+
+    for i in range(tile_count):
+        project(i)
+
+    near_src = near_out_ref.at[near_rows, :]
+    remote(near_src, near_src, es.at[0], er.at[0], e, other).wait_send()
+    remote(far_out_ref, far_out_ref, es.at[1], er.at[0], e, other).wait_send()
+    near_core(near_rows).wait_send()
+    far_core(far_rows).wait_send()
+    remote(near_ref, near_ref, ns.at[0], nr.at[0, 0], e, other).wait_send()
+    for h in range(1, n_y):
+        ref = piece_ref.at[far_rows, columns(t)]
+        remote(ref, ref, ys.at[h - 1], yr.at[h - 1, 0], e, other).wait_send()
+        forward_copy(far_rows, h).wait_send()
+        ref = stage_ref.at[h]
+        remote(ref, ref, bs.at[h - 1], br.at[h - 1, 0], e, other).wait_send()
+        w_plane(h).wait_send()
+    for h in range(n_y):
+        w_core(h).wait_send()
+    w_grouped().wait_send()
+    all_mixed().wait_send()
+    span(0, n_z, close_ends)
+    all_home().wait_recv()
     back = home_ref[...]
-    first, second = mm_tn(picks[0], back), mm_tn(picks[1], back)
+    first, second = mm_tn(picks_ref[0], back), mm_tn(picks_ref[1], back)
     for i in range(share // 128):
         at = slice(i * 128, (i + 1) * 128)
-        expert_ref[:, at] = bf(weights[0] * first[:, at] + weights[1] * second[:, at])
-    mixer_end(tile_count - 1)
-
-    def close(d):
-        ep_copy(d).wait_send()
-        core_copy(d).wait_send()
-        home_copy(d).wait_send()
-        for h in range(1, n_y):
-            y_copy(d, h).wait_send()
-            forward_copy(d, h).wait_send()
-
-    span(1, n_ep, close)
-
-    def close_back(d):
-        for h in range(1, n_y):
-            back_copy(d, h).wait_send()
-
-    span(0, n_ep, close_back)
-    for b in range(2):
-        for h in range(n_y):
-            near_copy(b, h).wait_send()
-    for i in range(tile_count):
-        for h in range(n_y):
-            mnear_copy(i, h).wait_send()
-        for h in range(1, n_y):
-            my_copy(i, h).wait_send()
-    span(0, n_z, close_ends)
+        expert_ref[:, at] = bf(weight_ref[0] * first[:, at] + weight_ref[1] * second[:, at])
+    all_home().wait_send()
 
 
 def local(
@@ -843,7 +905,6 @@
     slots = n_ep * capacity
     units = expert_gate_weight.shape[2]
     rows = positions // n_tp
-    tile_count = max(1, model // 512)
     out_weight = jnp.pad(mixer_output_weight, ((0, width - own_width), (0, 0)))
 
     def held(*shape):
@@ -877,7 +938,7 @@
         expert_down_weight,
     )
     in_vmem, in_hbm = pl.BlockSpec(memory_space=pltpu.VMEM), pl.BlockSpec(memory_space=pltpu.HBM)
-    one, many = sems(n_ep), sems(n_y, n_ep)
+    one, hops = sems(n_ep), sems(n_y - 1)
     mixer_out, expert_out = pl.pallas_call(
         functools.partial(whole_kernel, group),
         out_shape=(held(rows, model), held(tokens, share)),
@@ -885,7 +946,7 @@
         out_specs=[in_vmem] * 2,
         scratch_shapes=[held(positions, width)] * 6
         + [
-            held(width, model),
+            held(n_tp * width, model),
             held(tokens, model),
             single(1, width),
             single(1, width),
@@ -899,34 +960,37 @@
             single(positions, width),
             held(tokens, model),
             held(slots, tokens),
-            held(slots, share),
+            held(slots // 2, model // 2),
+            held(slots // 2, share),
+            held(2, slots, tokens),
+            single(2, tokens, 128),
             held(slots, model),
             single(positions, width),
             held(positions, width),
             held(n_ep, pairs * 2 * HEAD_DIM, PAIR),
             single(pairs, 2 * PAIR, PAIR),
             held(positions, width),
-            held(positions, model),
+            held(n_tp, rows, width),
             held(model, units),
             held(model, units),
             held(units, model),
             held(slots // 2, units),
+            single(slots // 2, units),
+            single(slots // 2, units),
             held(slots, model),
         ]
         + [held(n_y, slots, share)] * 3
         + [held(slots, share)] * 2
-        + [held(tile_count, n_y, rows, model // tile_count)] * 3
         + [sems(16)]
-        + [sems(max(1, units // 256))] * 2
-        + [sems(max(1, model // 512))]
-        + [one] * 4
-        + [many] * 4
+        + [sems(1)] * 3
+        + [sems(2), one, sems(2), sems(2)]
+        + [hops, sems(n_y - 1, n_ep // 2), hops, hops]
         + [sems(n_ep // n_x)] * 2
-        + [sems(n_x, n_ep // n_x)] * 2
-        + [sems(2, n_y)] * 2
-        + [many] * 2
-        + [one] * 2
-        + [sems(tile_count, n_y)] * 4,
+        + [sems(n_x - 1, n_ep // n_x)] * 2
+        + [sems(1), sems(2, n_y)]
+        + [hops, sems(n_y - 1, n_ep)]
+        + [sems(1)] * 2
+        + [hops, hops, sems(1), sems(1), sems(n_y), sems(n_y), sems(1), sems(1)],
         compiler_params=pltpu.CompilerParams(
             collective_id=0, has_side_effects=True, vmem_limit_bytes=VMEM_LIMIT
         ),

time: 52.5 us -> 49.4 us (0.941)
  the two profiles are of different devices: /device:TPU:0 before, /device:TPU:27 now
where the time goes in v3:
time: 49.4 us; the launch traced here: 49.2 us
  Pallas kernels  47.2 us (96%)
  local copies, waits for them, and re-layouts  1.45 us (3%)
  between operations  0.65 us (1%)
    pallas_call x1, Pallas kernels, local(): pl.pallas_call(functools.partial(whole_kernel, group), out_shape=(held(ro...  47.2 us
    unnamed x2, local copies, waits for them, and re-layouts  1.45 us

profile of v3, /device:TPU:27, one launch (start us, length us, event | category | flops | bytes accessed | tf_op | source)
XLA Modules:
  0.0 49.2 jit_solution(18100871836497863873)
XLA Ops:
  0.6 47.2 %shard_map.194 = (bf16[128,2048]{1,0:T(8,128)(2,1)S(1)}, bf16[128,512]{1,0:T(8,128)(2,1)S(1)}) custom-call(bf16[512,256]{1,0:T(8,128)(2,1)} %r_hbm.1, bf16[512,256]{1,0:T(8,128)(2,1)} %k_hbm.1, bf16[512,256]{1,0:T(8,128)(2,1)} %v_hbm.1, bf16[512,256]{1,0:T(8,128)(2,1)} %d_hbm.1, bf16[512,256]{1,0:T(8,128)(2,1)} %a_hbm.1, bf16[512,256]{1,0:T(8,128)(2,1)} %gate_in_hbm.1, ...), custom_call_target="tpu_custom_call" | custom-call | tf_op jit(solution)/shard_map/pallas_call | solution.py:942
  47.8 0.8 %copy.23 = bf16[128,2048]{1,0:T(8,128)(2,1)} copy(bf16[128,2048]{1,0:T(8,128)(2,1)S(1)} %get-tuple-element.2) | data formatting | bytes 1048576
  48.6 0.7 %copy.24 = bf16[128,512]{1,0:T(8,128)(2,1)} copy(bf16[128,512]{1,0:T(8,128)(2,1)S(1)} %get-tuple-element.3) | data formatting | bytes 262144

commit v4 on v3

--- a/solution.py
+++ b/solution.py
@@ -197,7 +197,7 @@
         ends_ref[p * 2 * C + C : (p + 1) * 2 * C] = bf(m[:C] + m[C:])
 
 
-def join_kernel(axis, all_ref, out_ref, reach_ref, gate_ref, gain_ref, mixed_ref):
+def join_kernel(axis, all_ref, out_ref, reach_ref, gate_ref, gain_ref, mixed_ref, owners, done):
     devices, place = lax.axis_size(axis), lax.axis_index(axis)
     width = out_ref.shape[1]
     pairs = width // PAIR
@@ -217,16 +217,22 @@
         return tuple(new)
 
     states = lax.fori_loop(0, place, hop, tuple(states))
+    rows = out_ref.shape[0] // len(owners)
+    moves = []
     for p in range(pairs):
-        lanes = slice(p * PAIR, (p + 1) * PAIR)
         s = bf(states[p])
-        s = jnp.concatenate([s, s], axis=0) * own_bf
-        head = out_ref[:, lanes] + mm_nt(reach_ref[:, lanes], s)
-        centred = head - sum_right(head, mean_bf)
-        spread = sum_right(centred * centred, mean_bf)
-        normed = centred * lax.rsqrt(spread + group_eps)
-        gate = logistic(gate_ref[:, lanes].astype(jnp.float32))
-        mixed_ref[:, lanes] = bf(normed * gain_ref[:, lanes] * gate)
+        moves.append(jnp.concatenate([s, s], axis=0) * own_bf)
+    for i, owner in enumerate(owners):
+        at = pl.ds(pl.multiple_of(owner * rows, rows), rows)
+        for p in range(pairs):
+            lanes = slice(p * PAIR, (p + 1) * PAIR)
+            head = out_ref[at, lanes] + mm_nt(reach_ref[at, lanes], moves[p])
+            centred = head - sum_right(head, mean_bf)
+            spread = sum_right(centred * centred, mean_bf)
+            normed = centred * lax.rsqrt(spread + group_eps)
+            gate = logistic(gate_ref[at, lanes].astype(jnp.float32))
+            mixed_ref[at, lanes] = bf(normed * gain_ref[:, lanes] * gate)
+        done(i)
 
 
 def place_of():
@@ -369,6 +375,7 @@
     wyr,
     wgs,
     wgr,
+    wzr,
     wcs,
     wcr,
     xs,
@@ -562,25 +569,31 @@
         home_copy(d).start()
 
     tile_count = model // wide_model
-    part_rows = width // half
-    part_at = lax.rem(e, half)
+    part_rows = width // (2 * n_x)
 
     def source_of(h):
         return 2 * lax.rem(y - h + n_y, n_y) + core
 
-    def shard_part(index):
-        return pl.ds(pl.multiple_of(index * width + part_at * part_rows, part_rows), part_rows)
+    def part(index, place):
+        return pl.ds(pl.multiple_of(index * width + place * part_rows, part_rows), part_rows)
+
+    own_part = lax.rem(e, 2 * n_x)
+    pair_part = lax.rem(own_part + n_x, 2 * n_x)
 
     def w_plane(h):
-        ref = w_ref.at[shard_part(t), :]
+        ref = w_ref.at[part(t, own_part), :]
         return remote(ref, ref, wys.at[h - 1], wyr.at[h - 1], e, 2 * peer_y(h) + core)
 
-    def w_group(h, k):
-        ref = w_ref.at[shard_part(source_of(h)), :]
+    def w_pair(h):
+        ref = w_ref.at[part(source_of(h), own_part), :]
+        return remote(ref, ref, wgs.at[0], wzr.at[h - 1], partner(n_x), t)
+
+    def w_line(h, place, k):
+        ref = w_ref.at[part(source_of(h), place), :]
         return remote(ref, ref, wgs.at[0], wgr.at[0], partner(k), t)
 
-    def w_grouped():
-        ref = w_ref.at[: (n_y - 1) * (half - 1) * part_rows, :]
+    def w_rows(count):
+        ref = w_ref.at[: (n_y - 1) * count * part_rows, :]
         return remote(ref, ref, wgs.at[0], wgr.at[0], partner(1), t)
 
     def w_core(h):
@@ -590,10 +603,15 @@
     def share_w():
         for h in range(1, n_y):
             w_plane(h).wait_recv()
-            span(1, half, lambda k: w_group(h, k).start())
-
-    def mixed_copy(j):
-        to = lax.rem(t + j, n_tp)
+            w_pair(h).start()
+            span(1, n_x, lambda k: w_line(h, own_part, k).start())
+
+    def share_pair_w():
+        for h in range(1, n_y):
+            w_pair(h).wait_recv()
+            span(1, n_x, lambda k: w_line(h, pair_part, k).start())
+
+    def mixed_copy(to):
         src = mixed_ref.at[pl.ds(pl.multiple_of(to * rows, rows), rows), :]
         return remote(src, mixed_all_ref.at[t], xs.at[0], xr.at[0], e, to)
 
@@ -650,14 +668,20 @@
         if b == 0:
             pltpu.make_async_copy(down_hbm.at[0], down_ref, down_sem.at[0]).wait()
 
-        def tile(i):
-            h = n_y - 1 - i % n_y
-            index = 2 * peer_y(h) + (1 - core if i < n_y else core)
+        def tile(h, ours):
+            index = 2 * peer_y(h) + (core if ours else 1 - core)
             part_ref[at, columns(index)] = bf(mm(hidden_ref[...], down_ref[:, columns(index)]))
-            if i < n_y:
-                near_copy(b, h).start()
-
-        tiles(n_tp, tile, hooks)
+
+        for h in range(n_y - 1, 0, -1):
+            tile(h, False)
+            near_copy(b, h).start()
+        for hook in hooks:
+            hook()
+        for h in range(n_y - 1, 0, -1):
+            tile(h, True)
+        tile(0, False)
+        tile(0, True)
+        near_copy(b, 0).start()
 
     for copy in loads:
         copy.start()
@@ -771,7 +795,9 @@
     near_core(near_rows).wait_recv()
     relays = [lambda i=i: relay_ends(i) for i in range(1, n_z)]
     widen_near({2: [far_unit(2, far_arrived)], 3: [far_unit(0, pass_on)]})
-    narrow(0, {0: [far_unit(1, pass_on)], 1: [far_unit(3, far_arrived)], 3: [far_unit(2, pass_on)]})
+    far_unit(1, pass_on)()
+    narrow(0, [far_unit(3, far_arrived)])
+    far_unit(2, pass_on)()
     add_near(0)
     for copy in loads[11:12] + loads[13:]:
         copy.wait()
@@ -807,23 +833,29 @@
     near_copy(0, 0).wait_recv()
     gathered()
     last = z == n_z - 1
-    widen_far_end({1: [lambda i=i: relay_ends(i, ~last) for i in range(2, 3)]})
-    narrow(1, {})
+    passing = [lambda i=i: relay_ends(i, ~last) for i in range(2, min(3, n_z))]
+    widen_far_end({1: passing})
+    late = [lambda i=i: relay_ends(i, last if i < 3 else True) for i in range(2, n_z)]
+    narrow(1, late + [share_pair_w])
     add_near(1)
     span(1, half, go_home)
     near_copy(1, 0).wait_recv()
     unit(4, go_home)()
-    for i in range(2, n_z):
-        relay_ends(i, last if i < 3 else True)
     for u in range(5, 8):
         unit(u, go_home)()
     home_ref[block(e), :] = add_far(0)
     span(0, n_z, collect_ends)
-    join_kernel("ep", every_ref, out_ref, reach_ref, gate_in_ref, gain_ref, mixed_ref)
-    for j in range(1, n_tp):
-        mixed_copy(j).start()
+    owners = [2 * peer_y(h) + c for h in range(1, n_y) for c in (core, 1 - core)] + [other, t]
+
+    def joined(i):
+        if i + 1 < n_tp:
+            mixed_copy(owners[i]).start()
+
+    join_kernel(
+        "ep", every_ref, out_ref, reach_ref, gate_in_ref, gain_ref, mixed_ref, owners, joined
+    )
     mixed_all_ref[t] = mixed_ref[pl.ds(pl.multiple_of(t * rows, rows), rows), :]
-    w_grouped().wait_recv()
+    w_rows(2 * n_x - 2).wait_recv()
     for h in range(1, n_y):
         w_core(h).start()
     all_mixed().wait_recv()
@@ -853,7 +885,7 @@
         w_plane(h).wait_send()
     for h in range(n_y):
         w_core(h).wait_send()
-    w_grouped().wait_send()
+    w_rows(2 * n_x - 1).wait_send()
     all_mixed().wait_send()
     span(0, n_z, close_ends)
     all_home().wait_recv()
@@ -990,7 +1022,7 @@
         + [sems(1), sems(2, n_y)]
         + [hops, sems(n_y - 1, n_ep)]
         + [sems(1)] * 2
-        + [hops, hops, sems(1), sems(1), sems(n_y), sems(n_y), sems(1), sems(1)],
+        + [hops, hops, sems(1), sems(1), hops, sems(n_y), sems(n_y), sems(1), sems(1)],
         compiler_params=pltpu.CompilerParams(
             collective_id=0, has_side_effects=True, vmem_limit_bytes=VMEM_LIMIT
         ),

time: 49.4 us -> 47.2 us (0.955)
  the two profiles are of different devices: /device:TPU:27 before, /device:TPU:0 now
where the time goes in v4:
time: 47.2 us; the launch traced here: 46.6 us
  Pallas kernels  44.5 us (94%)
  local copies, waits for them, and re-layouts  1.45 us (3%)
  between operations  0.65 us (1%)
    pallas_call x1, Pallas kernels, local(): pl.pallas_call(functools.partial(whole_kernel, group), out_shape=(held(ro...  44.5 us
    unnamed x2, local copies, waits for them, and re-layouts  1.45 us

profile of v4, /device:TPU:0, one launch (start us, length us, event | category | flops | bytes accessed | tf_op | source)
XLA Modules:
  0.0 46.6 jit_solution(16619446155635053219)
XLA Ops:
  0.6 44.5 %shard_map.194 = (bf16[128,2048]{1,0:T(8,128)(2,1)S(1)}, bf16[128,512]{1,0:T(8,128)(2,1)S(1)}) custom-call(bf16[512,256]{1,0:T(8,128)(2,1)} %r_hbm.1, bf16[512,256]{1,0:T(8,128)(2,1)} %k_hbm.1, bf16[512,256]{1,0:T(8,128)(2,1)} %v_hbm.1, bf16[512,256]{1,0:T(8,128)(2,1)} %d_hbm.1, bf16[512,256]{1,0:T(8,128)(2,1)} %a_hbm.1, bf16[512,256]{1,0:T(8,128)(2,1)} %gate_in_hbm.1, ...), custom_call_target="tpu_custom_call" | custom-call | tf_op jit(solution)/shard_map/pallas_call | solution.py:974
  45.1 0.8 %copy.23 = bf16[128,2048]{1,0:T(8,128)(2,1)} copy(bf16[128,2048]{1,0:T(8,128)(2,1)S(1)} %get-tuple-element.2) | data formatting | bytes 1048576
  45.9 0.7 %copy.24 = bf16[128,512]{1,0:T(8,128)(2,1)} copy(bf16[128,512]{1,0:T(8,128)(2,1)S(1)} %get-tuple-element.3) | data formatting | bytes 262144

commit v5 on v4

--- a/solution.py
+++ b/solution.py
@@ -197,7 +197,7 @@
         ends_ref[p * 2 * C + C : (p + 1) * 2 * C] = bf(m[:C] + m[C:])
 
 
-def join_kernel(axis, all_ref, out_ref, reach_ref, gate_ref, gain_ref, mixed_ref, owners, done):
+def join_kernel(axis, all_ref, out_ref, reach_ref, gate_ref, gain_ref, mixed_ref, planes, done):
     devices, place = lax.axis_size(axis), lax.axis_index(axis)
     width = out_ref.shape[1]
     pairs = width // PAIR
@@ -217,13 +217,13 @@
         return tuple(new)
 
     states = lax.fori_loop(0, place, hop, tuple(states))
-    rows = out_ref.shape[0] // len(owners)
+    rows = out_ref.shape[0] // len(planes)
     moves = []
     for p in range(pairs):
         s = bf(states[p])
         moves.append(jnp.concatenate([s, s], axis=0) * own_bf)
-    for i, owner in enumerate(owners):
-        at = pl.ds(pl.multiple_of(owner * rows, rows), rows)
+    for i, plane in enumerate(planes):
+        at = pl.ds(pl.multiple_of(plane * rows, rows), rows)
         for p in range(pairs):
             lanes = slice(p * PAIR, (p + 1) * PAIR)
             head = out_ref[at, lanes] + mm_nt(reach_ref[at, lanes], moves[p])
@@ -400,7 +400,9 @@
     def shard(index):
         return pl.ds(pl.multiple_of(index * width, width), width)
 
-    inputs = [(routes_hbm, routes_ref), (norm_gain_hbm, norm_gain_ref), (x_hbm, x_ref)]
+    x_rows = [slice(i * tokens // 4, (i + 1) * tokens // 4) for i in range(4)]
+    inputs = [(routes_hbm, routes_ref), (norm_gain_hbm, norm_gain_ref)]
+    inputs += [(x_hbm.at[at, :], x_ref.at[at, :]) for at in x_rows]
     inputs += [(extra_hbm, extra_in_ref), (d_off_hbm, d_off_ref), (a_off_hbm, a_off_ref)]
     inputs += [(k_hbm, k_ref), (a_hbm, a_ref), (d_hbm, d_ref), (r_hbm, r_ref), (v_hbm, v_ref)]
     inputs += [(gate_in_hbm, gate_in_ref), (out_weight_hbm, w_ref.at[shard(t), :]), (gain_hbm, gain_ref)]
@@ -600,16 +602,35 @@
         ref = w_ref.at[shard(source_of(h)), :]
         return remote(ref, ref, wcs.at[h], wcr.at[h], e, other)
 
+    def w_core_part(h, place):
+        ref = w_ref.at[part(source_of(h), place), :]
+        return remote(ref, ref, wcs.at[h], wcr.at[h], e, other)
+
     def share_w():
         for h in range(1, n_y):
             w_plane(h).wait_recv()
             w_pair(h).start()
             span(1, n_x, lambda k: w_line(h, own_part, k).start())
-
-    def share_pair_w():
+            w_core_part(h, own_part).start()
+
+    def share_pair_w(wanted):
+        @pl.when(wanted)
+        def _():
+            for h in range(1, n_y):
+                w_pair(h).wait_recv()
+                span(1, n_x, lambda k: w_line(h, pair_part, k).start())
+                w_core_part(h, pair_part).start()
+
+    def share_line_w():
+        w_rows(2 * n_x - 2).wait_recv()
         for h in range(1, n_y):
-            w_pair(h).wait_recv()
-            span(1, n_x, lambda k: w_line(h, pair_part, k).start())
+            for shift in (0, n_x):
+
+                def one(k):
+                    place = lax.rem(partner(k) + shift, 2 * n_x)
+                    w_core_part(h, place).start()
+
+                span(1, n_x, one)
 
     def mixed_copy(to):
         src = mixed_ref.at[pl.ds(pl.multiple_of(to * rows, rows), rows), :]
@@ -683,13 +704,8 @@
         tile(0, True)
         near_copy(b, 0).start()
 
-    for copy in loads:
+    for copy in loads[:6]:
         copy.start()
-    for i in range(units // wide_units):
-        for copy in gate_copy(i):
-            copy.start()
-    for i in range(model // wide_model):
-        down_copy(i).start()
     everyone_here = meet()
 
     order = flag(iota((tokens, tokens), 0) < iota((tokens, tokens), 1))
@@ -705,7 +721,15 @@
     level = iota((capacity, tokens), 0).astype(jnp.float32)
     for j in range(experts):
         place_ref[j * capacity : (j + 1) * capacity] = bf(flag(level == rank[j : j + 1, :]))
-    loads[2].wait()
+    for copy in loads[2:6]:
+        copy.wait()
+    for copy in loads[6:]:
+        copy.start()
+    for i in range(units // wide_units):
+        for copy in gate_copy(i):
+            copy.start()
+    for i in range(model // wide_model):
+        down_copy(i).start()
     step_rows = 32
     for i in range(tokens // step_rows):
         at = slice(i * step_rows, (i + 1) * step_rows)
@@ -736,11 +760,11 @@
         at = slice(i * wide_model, (i + 1) * wide_model)
         piece_ref[:capacity, at] = bf(mm(place_ref[block(e), :], normed_ref[:, at]))
 
-    loads[12].wait()
+    loads[15].wait()
     for h in range(1, n_y):
         w_plane(h).start()
     w_core(0).start()
-    for copy in loads[3:11]:
+    for copy in loads[6:14]:
         copy.wait()
     heads, pairs = extra_in_ref.shape[0], chain_ref.shape[0]
     exact = extra_in_ref[...]
@@ -791,15 +815,14 @@
     span(1, half, near_arrived)
     far_unit(0, far_arrived)()
     far_unit(1, far_arrived)()
-    share_w()
     near_core(near_rows).wait_recv()
     relays = [lambda i=i: relay_ends(i) for i in range(1, n_z)]
-    widen_near({2: [far_unit(2, far_arrived)], 3: [far_unit(0, pass_on)]})
+    widen_near({0: [share_w], 2: [far_unit(2, far_arrived)], 3: [far_unit(0, pass_on)]})
     far_unit(1, pass_on)()
     narrow(0, [far_unit(3, far_arrived)])
     far_unit(2, pass_on)()
     add_near(0)
-    for copy in loads[11:12] + loads[13:]:
+    for copy in loads[14:15] + loads[16:]:
         copy.wait()
 
     normed = normed_ref[...]
@@ -824,6 +847,7 @@
         for j in range(experts):
             at = slice(j * capacity, (j + 1) * capacity)
             picks_ref[k, at] = place_ref[at] * bf(flag(own_routes[k : k + 1, :] == j))
+    last = z == n_z - 1
     far_core(far_rows).wait_recv()
     widen_far_begin()
     for relay in relays[:1]:
@@ -832,12 +856,14 @@
         far_unit(3, pass_on)()
     near_copy(0, 0).wait_recv()
     gathered()
-    last = z == n_z - 1
     passing = [lambda i=i: relay_ends(i, ~last) for i in range(2, min(3, n_z))]
     widen_far_end({1: passing})
     late = [lambda i=i: relay_ends(i, last if i < 3 else True) for i in range(2, n_z)]
-    narrow(1, late + [share_pair_w])
+    narrow(1, late[:1] + [lambda: share_pair_w(~last)])
     add_near(1)
+    for relay in late[1:]:
+        relay()
+    share_pair_w(last)
     span(1, half, go_home)
     near_copy(1, 0).wait_recv()
     unit(4, go_home)()
@@ -845,19 +871,18 @@
         unit(u, go_home)()
     home_ref[block(e), :] = add_far(0)
     span(0, n_z, collect_ends)
-    owners = [2 * peer_y(h) + c for h in range(1, n_y) for c in (core, 1 - core)] + [other, t]
+    planes = [peer_y(h) for h in range(1, n_y)] + [y]
 
     def joined(i):
-        if i + 1 < n_tp:
-            mixed_copy(owners[i]).start()
+        if i + 1 < n_y:
+            mixed_copy(2 * planes[i] + core).start()
+        mixed_copy(2 * planes[i] + 1 - core).start()
 
     join_kernel(
-        "ep", every_ref, out_ref, reach_ref, gate_in_ref, gain_ref, mixed_ref, owners, joined
+        "ep", every_ref, out_ref, reach_ref, gate_in_ref, gain_ref, mixed_ref, planes, joined
     )
     mixed_all_ref[t] = mixed_ref[pl.ds(pl.multiple_of(t * rows, rows), rows), :]
-    w_rows(2 * n_x - 2).wait_recv()
-    for h in range(1, n_y):
-        w_core(h).start()
+    share_line_w()
     all_mixed().wait_recv()
     for h in range(n_y):
         w_core(h).wait_recv()
@@ -895,6 +920,37 @@
         at = slice(i * 128, (i + 1) * 128)
         expert_ref[:, at] = bf(weight_ref[0] * first[:, at] + weight_ref[1] * second[:, at])
     all_home().wait_send()
+
+
+def leave_kernel(mixer_ref, expert_ref, mixer_hbm, expert_hbm, sem):
+    parts = 4
+    rows = mixer_ref.shape[0] // parts
+    copies = []
+    for i in range(parts):
+        at = slice(i * rows, (i + 1) * rows)
+        copies.append(pltpu.make_async_copy(mixer_ref.at[at, :], mixer_hbm.at[at, :], sem.at[i]))
+    copies.append(pltpu.make_async_copy(expert_ref, expert_hbm, sem.at[parts]))
+    for copy in copies:
+        copy.start()
+    for copy in copies:
+        copy.wait()
+
+
+def leave(mixer_out, expert_out):
+    return pl.pallas_call(
+        leave_kernel,
+        out_shape=(
+            jax.ShapeDtypeStruct(mixer_out.shape, mixer_out.dtype),
+            jax.ShapeDtypeStruct(expert_out.shape, expert_out.dtype),
+        ),
+        in_specs=[pl.BlockSpec(memory_space=pltpu.VMEM)] * 2,
+        out_specs=[pl.BlockSpec(memory_space=pltpu.HBM)] * 2,
+        scratch_shapes=[pltpu.SemaphoreType.DMA((5,))],
+        compiler_params=pltpu.CompilerParams(vmem_limit_bytes=1 << 20),
+    )(
+        pltpu.with_memory_space_constraint(mixer_out, pltpu.VMEM),
+        pltpu.with_memory_space_constraint(expert_out, pltpu.VMEM),
+    )
 
 
 def local(
@@ -1013,7 +1069,7 @@
         ]
         + [held(n_y, slots, share)] * 3
         + [held(slots, share)] * 2
-        + [sems(16)]
+        + [sems(19)]
         + [sems(1)] * 3
         + [sems(2), one, sems(2), sems(2)]
         + [hops, sems(n_y - 1, n_ep // 2), hops, hops]
@@ -1029,7 +1085,7 @@
     )(
         *(pltpu.with_memory_space_constraint(x, pltpu.HBM) for x in operands)
     )
-    return mixer_out, expert_out
+    return leave(mixer_out, expert_out)
 
 
 def solution(mesh):

time: 47.2 us -> 46.2 us (0.979)
  local copies, waits for them, and re-layouts: 1.45 us -> 0 us
  Pallas kernels: 44.5 us -> 45.4 us
    unnamed x2 -> x0, local copies, waits for them, and re-layouts: 1.45 us -> none
    pallas_call x0 -> x1, Pallas kernels: none -> 0.87 us  [leave(): pl.pallas_call(leave_kernel, out_shape=(jax.ShapeDtypeStruct(mixer_out.sh...]
where the time goes in v5:
time: 46.2 us; the launch traced here: 46 us
  Pallas kernels  45.4 us (98%)
  between operations  0.65 us (1%)
    pallas_call x1, Pallas kernels, local(): pl.pallas_call(functools.partial(whole_kernel, group), out_shape=(held(ro...  44.5 us

profile of v5, /device:TPU:0, one launch (start us, length us, event | category | flops | bytes accessed | tf_op | source)
XLA Modules:
  0.0 46.0 jit_solution(14224056668878060098)
XLA Ops:
  0.6 44.5 %shard_map.194 = (bf16[128,2048]{1,0:T(8,128)(2,1)S(1)}, bf16[128,512]{1,0:T(8,128)(2,1)S(1)}) custom-call(bf16[512,256]{1,0:T(8,128)(2,1)} %r_hbm.1, bf16[512,256]{1,0:T(8,128)(2,1)} %k_hbm.1, bf16[512,256]{1,0:T(8,128)(2,1)} %v_hbm.1, bf16[512,256]{1,0:T(8,128)(2,1)} %d_hbm.1, bf16[512,256]{1,0:T(8,128)(2,1)} %a_hbm.1, bf16[512,256]{1,0:T(8,128)(2,1)} %gate_in_hbm.1, ...), custom_call_target="tpu_custom_call" | custom-call | tf_op jit(solution)/shard_map/pallas_call | solution.py:1030
  45.2 0.9 %shard_map.195 = (bf16[128,2048]{1,0:T(8,128)(2,1)}, bf16[128,512]{1,0:T(8,128)(2,1)}) custom-call(bf16[128,2048]{1,0:T(8,128)(2,1)S(1)} %get-tuple-element.4.mixer_ref, bf16[128,512]{1,0:T(8,128)(2,1)S(1)} %get-tuple-element.5.expert_ref), custom_call_target="tpu_custom_call" | custom-call | tf_op jit(solution)/shard_map/pallas_call | solution.py:940

commit v6 on v5

--- a/solution.py
+++ b/solution.py
@@ -337,6 +337,7 @@
     chain_ref,
     mixed_ref,
     mixed_all_ref,
+    product_ref,
     gate_ref,
     up_ref,
     down_ref,
@@ -532,43 +533,52 @@
         src = part_ref.at[at, columns(2 * peer_y(h) + 1 - core)]
         return remote(src, near_ref.at[h, at, :], ns.at[0], nr.at[b, h], e, other)
 
-    def back_copy(d, h):
-        src = stage_ref.at[h, block(d), :]
-        dst = far_ref.at[h, block(d), :]
-        return remote(src, dst, bs.at[h - 1], br.at[h - 1, d], e, 2 * peer_y(h) + core)
-
-    def home_copy(d):
-        src, dst = final_ref.at[block(d), :], home_ref.at[block(e), :]
+    half_block = capacity // 2
+
+    def sub(i):
+        return pl.ds(pl.multiple_of(i * half_block, half_block), half_block)
+
+    def back_copy(i, h):
+        src = stage_ref.at[h, sub(i), :]
+        dst = far_ref.at[h, sub(i), :]
+        return remote(src, dst, bs.at[h - 1], br.at[h - 1, i], e, 2 * peer_y(h) + core)
+
+    def home_copy(i):
+        d, s = lax.div(i, 2), lax.rem(i, 2)
+        src, dst = final_ref.at[sub(i), :], home_ref.at[sub(2 * e + s), :]
         return remote(src, dst, hs.at[0], hr.at[0], partner(d), t)
 
     def all_home():
         src, dst = final_ref.at[capacity:, :], home_ref.at[capacity:, :]
         return remote(src, dst, hs.at[0], hr.at[0], partner(1), t)
 
-    def pair_sum(d, h):
-        return wide(part_ref[block(d), columns(2 * peer_y(h) + core)]) + wide(near_ref[h, block(d), :])
+    def pair_sum(i, h):
+        return wide(part_ref[sub(i), columns(2 * peer_y(h) + core)]) + wide(near_ref[h, sub(i), :])
 
     def add_near(b):
         for h in range(1, n_y):
             near_copy(b, h).wait_recv()
 
-        def one(d):
+        def one(i):
             for h in range(1, n_y):
-                stage_ref[h, block(d), :] = bf(pair_sum(d, h))
-                back_copy(d, h).start()
-
-        span(b * half, (b + 1) * half, one)
-
-    def add_far(d):
-        total = pair_sum(d, 0)
+                stage_ref[h, sub(i), :] = bf(pair_sum(i, h))
+                back_copy(i, h).start()
+
+        span(2 * b * half, 2 * (b + 1) * half, one)
+
+    def add_far(i):
+        total = pair_sum(i, 0)
         for h in range(1, n_y):
-            back_copy(d, h).wait_recv()
-            total = total + wide(far_ref[h, block(d), :])
+            back_copy(i, h).wait_recv()
+            total = total + wide(far_ref[h, sub(i), :])
         return bf(total)
 
     def go_home(d):
-        final_ref[block(d), :] = add_far(d)
-        home_copy(d).start()
+        def one(i):
+            final_ref[sub(i), :] = add_far(i)
+            home_copy(i).start()
+
+        span(2 * d, 2 * d + 2, one)
 
     tile_count = model // wide_model
     part_rows = width // (2 * n_x)
@@ -636,9 +646,18 @@
         src = mixed_ref.at[pl.ds(pl.multiple_of(to * rows, rows), rows), :]
         return remote(src, mixed_all_ref.at[t], xs.at[0], xr.at[0], e, to)
 
-    def all_mixed():
-        ref = mixed_all_ref.at[1:]
+    def mixed_core():
+        src = mixed_ref.at[pl.ds(pl.multiple_of(other * rows, rows), rows), :]
+        return remote(src, mixed_all_ref.at[t], xs.at[1], xr.at[1], e, other)
+
+    def mixed_planes():
+        ref = mixed_all_ref.at[: n_tp - 2]
         return remote(ref, ref, xs.at[0], xr.at[0], e, other)
+
+    def plane_product(plane, at):
+        held_rows = pl.ds(pl.multiple_of(plane * 2 * width, 2 * width), 2 * width)
+        left = jnp.concatenate([mixed_all_ref[2 * plane], mixed_all_ref[2 * plane + 1]], axis=1)
+        return mm(left, w_ref[held_rows, at])
 
     def tiles(count, body, hooks):
         for i in range(count):
@@ -869,31 +888,36 @@
     unit(4, go_home)()
     for u in range(5, 8):
         unit(u, go_home)()
-    home_ref[block(e), :] = add_far(0)
+    for i in range(2):
+        home_ref[sub(2 * e + i), :] = add_far(i)
     span(0, n_z, collect_ends)
     planes = [peer_y(h) for h in range(1, n_y)] + [y]
 
     def joined(i):
         if i + 1 < n_y:
             mixed_copy(2 * planes[i] + core).start()
-        mixed_copy(2 * planes[i] + 1 - core).start()
+            mixed_copy(2 * planes[i] + 1 - core).start()
+        else:
+            mixed_core().start()
 
     join_kernel(
         "ep", every_ref, out_ref, reach_ref, gate_in_ref, gain_ref, mixed_ref, planes, joined
     )
     mixed_all_ref[t] = mixed_ref[pl.ds(pl.multiple_of(t * rows, rows), rows), :]
+    tile_slices = [slice(i * wide_model, (i + 1) * wide_model) for i in range(tile_count)]
+    w_core(0).wait_recv()
+    mixed_core().wait_recv()
+    for at in tile_slices:
+        product_ref[:, at] = plane_product(y, at)
     share_line_w()
-    all_mixed().wait_recv()
-    for h in range(n_y):
+    mixed_planes().wait_recv()
+    for h in range(1, n_y):
         w_core(h).wait_recv()
-    mixed = jnp.concatenate([mixed_all_ref[j] for j in range(n_tp)], axis=1)
-
-    def project(i):
-        at = pl.ds(pl.multiple_of(i * wide_model, wide_model), wide_model)
-        mixer_ref[:, at] = bf(mm(mixed, w_ref[:, at]))
-
-    for i in range(tile_count):
-        project(i)
+    for at in tile_slices:
+        total = product_ref[:, at]
+        for h in range(1, n_y):
+            total = total + plane_product(peer_y(h), at)
+        mixer_ref[:, at] = bf(total)
 
     near_src = near_out_ref.at[near_rows, :]
     remote(near_src, near_src, es.at[0], er.at[0], e, other).wait_send()
@@ -911,7 +935,8 @@
     for h in range(n_y):
         w_core(h).wait_send()
     w_rows(2 * n_x - 1).wait_send()
-    all_mixed().wait_send()
+    mixed_planes().wait_send()
+    mixed_core().wait_send()
     span(0, n_z, close_ends)
     all_home().wait_recv()
     back = home_ref[...]
@@ -1059,6 +1084,7 @@
             single(pairs, 2 * PAIR, PAIR),
             held(positions, width),
             held(n_tp, rows, width),
+            single(rows, model),
             held(model, units),
             held(model, units),
             held(units, model),
@@ -1076,9 +1102,9 @@
         + [sems(n_ep // n_x)] * 2
         + [sems(n_x - 1, n_ep // n_x)] * 2
         + [sems(1), sems(2, n_y)]
-        + [hops, sems(n_y - 1, n_ep)]
+        + [hops, sems(n_y - 1, 2 * n_ep)]
         + [sems(1)] * 2
-        + [hops, hops, sems(1), sems(1), hops, sems(n_y), sems(n_y), sems(1), sems(1)],
+        + [hops, hops, sems(1), sems(1), hops, sems(n_y), sems(n_y), sems(2), sems(2)],
         compiler_params=pltpu.CompilerParams(
             collective_id=0, has_side_effects=True, vmem_limit_bytes=VMEM_LIMIT
         ),

time: 46.2 us -> 46 us (level)
  no operation moved by 1% of the time
where the time goes in v6:
time: 46 us; the launch traced here: 45.8 us
  Pallas kernels  45.1 us (98%)
  between operations  0.65 us (1%)
    pallas_call x1, Pallas kernels, local(): pl.pallas_call(functools.partial(whole_kernel, group), out_shape=(held(ro...  44.3 us

profile of v6, /device:TPU:0, one launch (start us, length us, event | category | flops | bytes accessed | tf_op | source)
XLA Modules:
  0.0 45.8 jit_solution(10140027040882470178)
XLA Ops:
  0.6 44.3 %shard_map.194 = (bf16[128,2048]{1,0:T(8,128)(2,1)S(1)}, bf16[128,512]{1,0:T(8,128)(2,1)S(1)}) custom-call(bf16[512,256]{1,0:T(8,128)(2,1)} %r_hbm.1, bf16[512,256]{1,0:T(8,128)(2,1)} %k_hbm.1, bf16[512,256]{1,0:T(8,128)(2,1)} %v_hbm.1, bf16[512,256]{1,0:T(8,128)(2,1)} %d_hbm.1, bf16[512,256]{1,0:T(8,128)(2,1)} %a_hbm.1, bf16[512,256]{1,0:T(8,128)(2,1)} %gate_in_hbm.1, ...), custom_call_target="tpu_custom_call" | custom-call | tf_op jit(solution)/shard_map/pallas_call | solution.py:1055
  44.9 0.9 %shard_map.195 = (bf16[128,2048]{1,0:T(8,128)(2,1)}, bf16[128,512]{1,0:T(8,128)(2,1)}) custom-call(bf16[128,2048]{1,0:T(8,128)(2,1)S(1)} %get-tuple-element.4.mixer_ref, bf16[128,512]{1,0:T(8,128)(2,1)S(1)} %get-tuple-element.5.expert_ref), custom_call_target="tpu_custom_call" | custom-call | tf_op jit(solution)/shard_map/pallas_call | solution.py:965

commit v7 on v6

--- a/solution.py
+++ b/solution.py
@@ -883,11 +883,18 @@
     for relay in late[1:]:
         relay()
     share_pair_w(last)
-    span(1, half, go_home)
+
+    def near_home(wanted):
+        @pl.when(wanted)
+        def _():
+            span(1, half, go_home)
+
+    near_home(~last)
     near_copy(1, 0).wait_recv()
     unit(4, go_home)()
     for u in range(5, 8):
         unit(u, go_home)()
+    near_home(last)
     for i in range(2):
         home_ref[sub(2 * e + i), :] = add_far(i)
     span(0, n_z, collect_ends)

time: 46 us -> 45.7 us (level)
  no operation moved by 1% of the time
where the time goes in v7:
time: 45.7 us; the launch traced here: 45.4 us
  Pallas kernels  44.8 us (98%)
  between operations  0.65 us (1%)
    pallas_call x1, Pallas kernels, local(): pl.pallas_call(functools.partial(whole_kernel, group), out_shape=(held(ro...  43.9 us

profile of v7, /device:TPU:0, one launch (start us, length us, event | category | flops | bytes accessed | tf_op | source)
XLA Modules:
  0.0 45.4 jit_solution(4533535771667688386)
XLA Ops:
  0.6 43.9 %shard_map.194 = (bf16[128,2048]{1,0:T(8,128)(2,1)S(1)}, bf16[128,512]{1,0:T(8,128)(2,1)S(1)}) custom-call(bf16[512,256]{1,0:T(8,128)(2,1)} %r_hbm.1, bf16[512,256]{1,0:T(8,128)(2,1)} %k_hbm.1, bf16[512,256]{1,0:T(8,128)(2,1)} %v_hbm.1, bf16[512,256]{1,0:T(8,128)(2,1)} %d_hbm.1, bf16[512,256]{1,0:T(8,128)(2,1)} %a_hbm.1, bf16[512,256]{1,0:T(8,128)(2,1)} %gate_in_hbm.1, ...), custom_call_target="tpu_custom_call" | custom-call | tf_op jit(solution)/shard_map/pallas_call | solution.py:1062
  44.5 0.9 %shard_map.195 = (bf16[128,2048]{1,0:T(8,128)(2,1)}, bf16[128,512]{1,0:T(8,128)(2,1)}) custom-call(bf16[128,2048]{1,0:T(8,128)(2,1)S(1)} %get-tuple-element.4.mixer_ref, bf16[128,512]{1,0:T(8,128)(2,1)S(1)} %get-tuple-element.5.expert_ref), custom_call_target="tpu_custom_call" | custom-call | tf_op jit(solution)/shard_map/pallas_call | solution.py:972
